TPU v7x, 256 devices: a whole 4x4x8 slice. The times are simulated.
256 devices in a mesh: ep: 128 (over z, y, x), tp: 2 (over core).
Axes of the slice: x: 4, y: 4, z: 8, core: 2. Of those that a mesh axis runs over, the one named last changes fastest.
Arguments:
- hidden: bfloat16 [2048, 2048], P('ep'), may hold values from -6 to 6
- attn_gain: bfloat16 [2048], replicated, may hold values from 0.099609375 to 1.8984375
- query_weight: bfloat16 [2048, 2048], P(None, 'tp'), may hold values from -0.125 to 0.125
- key_weight: bfloat16 [2048, 128], P(None, 'tp'), may hold values from -0.125 to 0.125
- value_weight: bfloat16 [2048, 128], P(None, 'tp'), may hold values from -0.125 to 0.125
- forget_weight: bfloat16 [2048, 32], P(None, 'tp'), may hold values from -0.125 to 0.125
- forget_bias: float32 [32], P('tp'), may hold values from -1 to 4
- cache_keys: bfloat16 [2048, 2, 64, 1024], P('ep', 'tp'), may hold values from -64 to 64
- cache_values: bfloat16 [2048, 2, 64, 1024], P('ep', 'tp'), may hold values from -6 to 6
- cache_logsum: float32 [2048, 32, 1024], P('ep', 'tp'), may hold values from -144 to 0, as said below
- lengths: int32 [2048], P('ep'), may hold values from 2 to 1023, as said below
- out_weight: bfloat16 [2048, 2048], P('ep'), may hold values from -0.125 to 0.125
- ffn_gain: bfloat16 [2048], replicated, may hold values from 0.099609375 to 1.8984375
- expert_ids: int32 [2048, 6], P('ep'), may hold values from 0 to 127, all different within a row; in each aligned block of 16 rows (0 to 15, 16 to 31, ...) at most 2 rows name the same one
- expert_scores: float32 [2048, 6], P('ep'), may hold values from 0.1 to 1
- gate_weights: bfloat16 [128, 2048, 512], P('ep', None, 'tp'), may hold values from -0.125 to 0.125
- up_weights: bfloat16 [128, 2048, 512], P('ep', None, 'tp'), may hold values from -0.125 to 0.125
- down_weights: bfloat16 [128, 512, 2048], P('ep', 'tp'), may hold values from -0.25 to 0.25
Outputs:
- updated: bfloat16 [2048, 2048], P('ep')
- new_key: bfloat16 [2048, 2, 64], P('ep', 'tp')
- new_value: bfloat16 [2048, 2, 64], P('ep', 'tp')
- new_logsum: float32 [2048, 32], P('ep', 'tp')
Inputs may be any that keep to these rules, and one draw needn't show every extreme that they name: `cache_logsum`: non-increasing along the positions. The new token stands at position lengths; some sequence has 1023 cached positions. `expert_ids`: each row names 6 different experts; the rows of one index of ep name one expert at most 2 times.
All inputs are finite; a program needn't handle non-finite values.
Results may differ from a plain program's by a relative error of at most 0.006.
Values may be sent and summed in bfloat16 or wider, within the bound.
A program may use at most 64 MiB of HBM per device.

v0:
```python
import jax
import jax.numpy as jnp
from jax import lax
from jax.sharding import Mesh
from jax.sharding import PartitionSpec as P

HD = 64
TOP_K = 6
EP = ("ep_0", "ep_1", "ep_2")


epsilon = 1e-06


def gather_axes(array, axes, dim):
    if not axes:
        return array
    nearer = lax.all_gather(array, axes[-1], axis=dim, tiled=True)
    return gather_axes(nearer, axes[:-1], dim)


def from_everyone(array, axis):
    devices = lax.axis_size(axis)
    return lax.all_to_all(
        jnp.broadcast_to(array[None], (devices, *array.shape)), axis, 0, 0, tiled=True
    )


def over_copies(array, axis):
    everything = from_everyone(array, axis)
    return jnp.sum(everything, axis=0)


def in_blocks(array, dim, devices):
    before, after = (array.shape[:dim], array.shape[dim + 1 :])
    return jnp.moveaxis(array.reshape(*before, devices, -1, *after), dim, 0)


def sum_at_owner(array, axis, dim):
    blocks = in_blocks(array, dim, lax.axis_size(axis))
    arrived = lax.all_to_all(blocks, axis, split_axis=0, concat_axis=0, tiled=True)
    return arrived.astype(jnp.float32).sum(axis=0)


def root_norm(values_in, gain):
    floats = values_in.astype(jnp.float32)
    inv_root = lax.rsqrt(jnp.mean(floats * floats, axis=-1, keepdims=True) + epsilon)
    return floats * inv_root * gain.astype(jnp.float32)


def per_device(
    hidden,
    attn_gain,
    query_weight,
    key_weight,
    value_weight,
    forget_weight,
    forget_bias,
    cache_keys,
    cache_values,
    cache_logsum,
    lengths,
    out_weight,
    ffn_gain,
    expert_ids,
    expert_scores,
    gate_weights,
    up_weights,
    down_weights,
):
    rows_here = hidden.shape[0]
    query_heads = query_weight.shape[1] // HD
    key_heads = key_weight.shape[1] // HD
    group_size = query_heads // key_heads
    cache_len = cache_keys.shape[-1]
    score_scale = HD ** (-0.5)
    normed = root_norm(hidden, attn_gain).astype(jnp.bfloat16)
    queries = jnp.dot(normed, query_weight, preferred_element_type=jnp.float32).astype(jnp.bfloat16)
    key_new = (
        jnp.dot(normed, key_weight, preferred_element_type=jnp.float32)
        .astype(jnp.bfloat16)
        .reshape(rows_here, key_heads, HD)
    )
    value_new = (
        jnp.dot(normed, value_weight, preferred_element_type=jnp.float32)
        .astype(jnp.bfloat16)
        .reshape(rows_here, key_heads, HD)
    )
    log_forget = jax.nn.log_sigmoid(
        jnp.dot(normed, forget_weight, preferred_element_type=jnp.float32) + forget_bias
    )
    positions = jnp.arange(cache_len, dtype=jnp.int32)
    is_last = positions[None, :] == (lengths - 1)[:, None]
    new_logsum = jnp.sum(jnp.where(is_last[:, None, :], cache_logsum, 0.0), axis=-1) + log_forget
    grouped = queries.reshape(rows_here, key_heads, group_size, HD)
    scores = jnp.einsum("sgjd,sgdp->sgjp", grouped, cache_keys, preferred_element_type=jnp.float32)
    scores = scores.reshape(rows_here, query_heads, cache_len) * score_scale
    scores = scores + new_logsum[:, :, None] - cache_logsum
    is_live = positions[None, :] < lengths[:, None]
    scores = jnp.where(is_live[:, None, :], scores, -jnp.inf)
    own_score = (
        jnp.einsum("sgjd,sgd->sgj", grouped, key_new, preferred_element_type=jnp.float32).reshape(
            rows_here, query_heads
        )
        * score_scale
    )
    top_score = jnp.maximum(jnp.max(scores, axis=-1), own_score)
    past_exp = jnp.exp(scores - top_score[:, :, None])
    own_exp = jnp.exp(own_score - top_score)
    denominator = jnp.sum(past_exp, axis=-1) + own_exp
    past_weight = (past_exp / denominator[:, :, None]).astype(jnp.bfloat16)
    own_weight = (own_exp / denominator).astype(jnp.bfloat16)
    attended = jnp.einsum(
        "sgjp,sgdp->sgjd",
        past_weight.reshape(rows_here, key_heads, group_size, cache_len),
        cache_values,
        preferred_element_type=jnp.float32,
    )
    attended = (
        attended
        + own_weight.astype(jnp.float32).reshape(rows_here, key_heads, group_size)[:, :, :, None]
        * value_new.astype(jnp.float32)[:, :, None, :]
    )
    attended = attended.reshape(rows_here, query_heads * HD).astype(jnp.bfloat16)
    head_width = attended.shape[1]
    own_columns = lax.dynamic_slice_in_dim(
        out_weight, lax.axis_index("tp") * head_width, head_width, 1
    )
    partial_rows = lax.dot_general(
        gather_axes(attended, EP, 0),
        own_columns,
        (((1,), (1,)), ((), ())),
        preferred_element_type=jnp.float32,
    )
    projected = over_copies(partial_rows, "tp").astype(jnp.bfloat16)
    mixed = lax.all_to_all(projected, EP, split_axis=0, concat_axis=1, tiled=True)
    residual = hidden.astype(jnp.float32) + mixed.astype(jnp.float32)
    ffn_in = root_norm(residual, ffn_gain).astype(jnp.bfloat16)
    ep_size = lax.axis_size(EP)
    local_experts = gate_weights.shape[0]
    experts = ep_size * local_experts
    route_count = rows_here * TOP_K
    capacity = 2 * ((route_count + experts - 1) // experts)
    flat_ids = expert_ids.reshape(route_count)
    onehot = (flat_ids[:, None] == jnp.arange(experts, dtype=jnp.int32)[None, :]).astype(jnp.int32)
    running = jnp.cumsum(onehot, axis=0)
    slot_index = jnp.sum(running * onehot, axis=1) - 1
    target = flat_ids * capacity + slot_index
    dispatch_map = (
        target[:, None] == jnp.arange(experts * capacity, dtype=jnp.int32)[None, :]
    ).astype(jnp.bfloat16)
    route_rows = jnp.repeat(ffn_in, TOP_K, axis=0)
    outgoing = lax.dot_general(
        dispatch_map, route_rows, (((0,), (0,)), ((), ())), preferred_element_type=jnp.float32
    )
    outgoing = outgoing.astype(jnp.bfloat16).reshape(
        ep_size, local_experts, capacity, ffn_in.shape[1]
    )
    arrived = lax.all_to_all(outgoing, EP, split_axis=0, concat_axis=0, tiled=True)
    gate_act = jnp.einsum(
        "sekd,edf->sekf", arrived, gate_weights, preferred_element_type=jnp.float32
    )
    up_act = jnp.einsum("sekd,edf->sekf", arrived, up_weights, preferred_element_type=jnp.float32)
    hidden_act = (jax.nn.silu(gate_act) * up_act).astype(jnp.bfloat16)
    partial_out = jnp.einsum(
        "sekf,efd->sekd", hidden_act, down_weights, preferred_element_type=jnp.float32
    )
    half_sum = sum_at_owner(partial_out.astype(jnp.bfloat16), "tp", 3).astype(jnp.bfloat16)
    sent_back = lax.all_to_all(half_sum, EP, split_axis=0, concat_axis=0, tiled=True)
    share_width = sent_back.shape[-1]
    picked = jnp.dot(
        dispatch_map,
        sent_back.reshape(experts * capacity, share_width),
        preferred_element_type=jnp.float32,
    )
    route_weight = expert_scores / jnp.sum(expert_scores, axis=-1, keepdims=True)
    expert_mix = jnp.sum(
        picked.reshape(rows_here, TOP_K, share_width) * route_weight[:, :, None], axis=1
    )
    own_part = lax.dynamic_slice_in_dim(
        residual, lax.axis_index("tp") * share_width, share_width, 1
    )
    updated = lax.all_gather((own_part + expert_mix).astype(jnp.bfloat16), "tp", axis=1, tiled=True)
    return (updated, key_new, value_new, new_logsum)


def solution(mesh):
    split = Mesh(mesh.devices.reshape(8, 4, 4, mesh.shape["tp"]), ("ep_0", "ep_1", "ep_2", "tp"))
    in_specs = (
        P(EP, None),
        P(),
        P(None, "tp"),
        P(None, "tp"),
        P(None, "tp"),
        P(None, "tp"),
        P("tp"),
        P(EP, "tp", None, None),
        P(EP, "tp", None, None),
        P(EP, "tp", None),
        P(EP),
        P(EP, None),
        P(),
        P(EP, None),
        P(EP, None),
        P(EP, None, "tp"),
        P(EP, None, "tp"),
        P(EP, "tp", None),
    )
    out_specs = (P(EP, None), P(EP, "tp", None), P(EP, "tp", None), P(EP, "tp"))
    return jax.shard_map(
        per_device, mesh=split, in_specs=in_specs, out_specs=out_specs, check_vma=False
    )
```

profile of v0, /device:TPU:1, one launch (start us, length us, event | category | flops | bytes accessed | tf_op | source)
XLA Modules:
  0.0 228.6 jit_solution(2594349491238698761)
XLA Ops:
  7.2 0.0 copy-start
  7.2 0.0 all-gather.2.cloned.1.call-start
  7.2 0.8 broadcast_add_fusion.1
  8.0 0.7 iota_compare_fusion.4
  8.8 0.7 convert_element_type.92
  9.5 1.0 fusion.46
  10.5 0.0 copy-start.14
  10.5 3.0 %convolution_convert_fusion.2 = bf16[16,1024]{1,0:T(8,128)(2,1)S(1)} fusion(bf16[2048,1024]{1,0:T(8,128)(2,1)} %param.20, bf16[16,2048]{1,0:T(8,128)(2,1)} %param.18, f32[2048]{0:T(1024)S(1)} %convert_element_type.92, f32[16]{0:T(128)S(1)} %add_rsqrt_fusion.1), kind=kOutput, calls=%fused_computation.19 | convolution fusion | flops 67256320 | bytes 4300864 | tf_op jit(solution)/shard_map/dot_general | solution.py:78
  13.5 0.1 reshape.210
  13.6 0.1 iota_compare_fusion.3
  13.7 1.2 convolution_convert_fusion.4
  14.9 0.2 select_reduce_fusion
  15.1 0.1 fusion.59
  15.2 0.2 fusion.58
  15.5 0.0 copy-start.9
  15.5 0.0 copy-start.5
  15.5 0.5 fusion.69
  16.1 0.0 copy-done.9
  16.1 0.3 fusion.32
  16.4 0.0 copy-done.5
  16.5 0.8 fusion.70
  17.3 0.7 fusion.23
  18.0 0.1 convert_element_type.102
  18.2 10.3 %all_gather.12 = bf16[64,1024]{1,0:T(8,128)(2,1)S(1)} all-gather(bf16[16,1024]{1,0:T(8,128)(2,1)S(1)} %convert_element_type.102), channel_id=1, replica_groups=mesh['ep_0'=8,'ep_1'=4,'ep_2'=4,'tp'=2] {'ep_2'}, dimensions={0}, use_global_device_ids=true | all-gather | bytes 163840 | tf_op jit(solution)/shard_map/all_gather | solution.py:18
  28.5 11.1 %all_gather.13 = bf16[256,1024]{1,0:T(8,128)(2,1)} all-gather(bf16[64,1024]{1,0:T(8,128)(2,1)S(1)} %all_gather.12), channel_id=1, replica_groups=mesh['ep_0'=8,'ep_1'=4,'ep_2'=4,'tp'=2] {'ep_1'}, dimensions={0}, use_global_device_ids=true | all-gather | bytes 655360 | tf_op jit(solution)/shard_map/all_gather | solution.py:18
  39.6 0.0 all-gather.2.cloned.1.call-update
  39.7 0.1 copy.45
  39.7 0.1 eq.67
  39.8 0.1 fusion.54
  39.9 0.1 reduce_window_sum.11
  40.1 0.2 select_reduce_fusion.1
  40.2 61.5 %all-gather.2.cloned.1.call-done = bf16[2048,1024]{1,0:T(8,128)(2,1)} async-done(((bf16[256,1024]{1,0:T(8,128)(2,1)}), bf16[2048,1024]{1,0:T(8,128)(2,1)}) %all-gather.2.cloned.1.call-update) | async-done | bytes 4194320 | tf_op jit(solution)/shard_map/all_gather | solution.py:18
  101.8 3.4 %fusion.55 = f32[2048,16]{0,1:T(8,128)S(1)} fusion(bf16[2048,1024]{1,0:T(8,128)(2,1)} %all-gather.2.cloned.1.call-done, bf16[16,2048]{1,0:T(8,128)(2,1)S(1)} %copy-done.6, s32[]{:T(128)S(6)} %select_n.19), kind=kOutput, calls=%fused_computation.63 | convolution fusion | flops 67108864 | bytes 4358148 | tf_op jit(solution)/shard_map/dot_general | solution.py:129
  105.2 4.4 %all_to_all.30 = f32[2,2048,16]{1,2,0:T(8,128)S(1)} all-to-all(f32[2,2048,16]{1,2,0:T(8,128)S(1)} %broadcast_in_dim.28), channel_id=1, replica_groups=mesh['ep_0'=8,'ep_1'=4,'ep_2'=4,'tp'=2] {'tp'}, dimensions={0} | all-to-all | bytes 524288 | tf_op jit(solution)/shard_map/all_to_all | solution.py:24
  109.6 0.4 convert_element_type.104
  110.0 0.3 copy.72
  110.4 1.0 reshape.232
  111.4 11.1 %all-to-all-start.1 = ((bf16[128,2,128]{2,1,0:T(2,128)(2,1)}), bf16[128,2,128]{2,1,0:T(2,128)(2,1)S(1)}, u32[]{:S(2)}, u32[]{:S(2)}) async-start(bf16[128,2,128]{2,1,0:T(2,128)(2,1)} %reshape.232), calls=%async_computation.1 | async-start | bytes 131072 | tf_op jit(solution)/shard_map/all_to_all | solution.py:136
  122.5 10.7 %all-to-all-done.1 = bf16[128,2,128]{2,1,0:T(2,128)(2,1)S(1)} async-done(((bf16[128,2,128]{2,1,0:T(2,128)(2,1)}), bf16[128,2,128]{2,1,0:T(2,128)(2,1)S(1)}, u32[]{:S(2)}, u32[]{:S(2)}) %all-to-all-start.1) | async-done | bytes 65568 | tf_op jit(solution)/shard_map/all_to_all | solution.py:136
  133.2 1.1 reshape.233
  134.3 1.1 bitcast_convert_fusion
  135.5 0.3 copy.54
  135.8 0.1 multiply_reduce_fusion
  135.9 0.6 copy-done.3
  136.6 0.1 multiply_convert_fusion
  136.6 0.1 broadcast_in_dim.29
  136.7 0.1 reshape.213
  136.8 0.5 convolution_convert_fusion
  137.4 1.5 reshape.214
  138.9 34.3 %all_to_all.31 = bf16[128,1,2,2048]{3,2,1,0:T(2,128)(2,1)S(1)} all-to-all(bf16[128,1,2,2048]{3,2,1,0:T(2,128)(2,1)} %bitcast.107), channel_id=1, replica_groups=mesh['ep_0'=8,'ep_1'=4,'ep_2'=4,'tp'=2] {'ep_0','ep_1','ep_2'}, dimensions={0} | all-to-all | bytes 2097152 | tf_op jit(solution)/shard_map/all_to_all | solution.py:159
  173.2 0.7 convolution_bitcast_fusion.1
  173.9 3.8 %convolution_convert_fusion.1 = bf16[128,2,2048]{2,0,1:T(8,128)(2,1)} fusion(bf16[1,256,2048]{2,1,0:T(8,128)(2,1)} %param.35, bf16[1,2048,256]{2,1,0:T(8,128)(2,1)} %param.34, bf16[128,1,2,2048]{3,2,1,0:T(2,128)(2,1)S(1)} %all_to_all.31, f32[128,1,2,256]{3,0,2,1:T(8,128)S(1)} %convolution_bitcast_fusion.1), kind=kOutput, calls=%fused_computation.1 | convolution fusion | flops 537788416 | bytes 4456448 | tf_op jit(solution)/shard_map/sekf,efd->sekd/dot_general | solution.py:165
  177.8 1.3 copy.71
  179.1 8.6 %all_to_all.32 = bf16[2,128,1,2,1024]{4,1,3,2,0:T(8,128)(2,1)S(1)} all-to-all(bf16[2,128,1,2,1024]{4,1,3,2,0:T(8,128)(2,1)S(1)} %bitcast.108), channel_id=1, replica_groups=mesh['ep_0'=8,'ep_1'=4,'ep_2'=4,'tp'=2] {'tp'}, dimensions={0} | all-to-all | bytes 2097152 | tf_op jit(solution)/shard_map/all_to_all | solution.py:41
  187.7 1.1 reduce_sum.92
  188.8 2.4 %copy.51 = bf16[128,1,2,1024]{3,2,1,0:T(2,128)(2,1)} copy(bf16[128,1,2,1024]{3,0,2,1:T(8,128)(2,1)} %bitcast.109) | data formatting | bytes 1048576 | tf_op jit(solution)/shard_map/reduce_sum | solution.py:42
  191.3 6.2 %all-to-all-start.4 = ((bf16[128,1,2,1024]{3,2,1,0:T(2,128)(2,1)}), bf16[128,1,2,1024]{3,2,1,0:T(2,128)(2,1)S(1)}, u32[]{:S(2)}, u32[]{:S(2)}) async-start(bf16[128,1,2,1024]{3,2,1,0:T(2,128)(2,1)} %copy.51), calls=%async_computation.4 | async-start | bytes 1048576 | tf_op jit(solution)/shard_map/all_to_all | solution.py:169
  197.5 0.1 sub.33
  197.5 0.1 copy.46
  197.7 19.0 %all-to-all-done.4 = bf16[128,1,2,1024]{3,2,1,0:T(2,128)(2,1)S(1)} async-done(((bf16[128,1,2,1024]{3,2,1,0:T(2,128)(2,1)}), bf16[128,1,2,1024]{3,2,1,0:T(2,128)(2,1)S(1)}, u32[]{:S(2)}, u32[]{:S(2)}) %all-to-all-start.4) | async-done | bytes 524320 | tf_op jit(solution)/shard_map/all_to_all | solution.py:169
  216.6 0.2 reshape.230
  216.8 0.3 fusion.17
  217.1 4.0 %all_gather.15 = bf16[16,2048]{1,0:T(8,128)(2,1)S(1)} all-gather(bf16[16,1024]{1,0:T(8,128)(2,1)S(1)} %add_convert_fusion), channel_id=1, replica_groups=mesh['ep_0'=8,'ep_1'=4,'ep_2'=4,'tp'=2] {'tp'}, dimensions={1}, use_global_device_ids=true | all-gather | bytes 98304 | tf_op jit(solution)/shard_map/all_gather | solution.py:183
  221.1 0.6 copy.74
  (37 shorter events, 0.2 us)
Async XLA Ops:
  7.2 8.3 %copy-start = (bf16[16,1,64,1024]{3,2,1,0:T(8,128)(2,1)S(1)}, bf16[16,1,64,1024]{3,2,1,0:T(8,128)(2,1)}, u32[]{:S(2)}) copy-start(bf16[16,1,64,1024]{3,2,1,0:T(8,128)(2,1)} %param.25) | copy-start | bytes 6291460
  7.2 94.6 %all-gather.2.cloned.1.call-start = ((), (), s32[]{:S(2)}) async-start(), calls=%async_computation.5 | async-start | bytes 4718592 | tf_op jit(solution)/shard_map/all_gather | solution.py:18
  10.4 3.3 %copy-start.2 = (bf16[16,2048]{1,0:T(8,128)(2,1)S(1)}, bf16[16,2048]{1,0:T(8,128)(2,1)}, u32[]{:S(2)}) copy-start(bf16[16,2048]{1,0:T(8,128)(2,1)} %param.18) | copy-start | bytes 196612
  10.4 4.4 %copy-start.1 = (f32[16,16,1024]{2,1,0:T(8,128)S(1)}, f32[16,16,1024]{2,1,0:T(8,128)}, u32[]{:S(2)}) copy-start(f32[16,16,1024]{2,1,0:T(8,128)} %param.27) | copy-start | bytes 3145732
  10.5 4.8 %copy-start.13 = (bf16[2048,16]{0,1:T(8,128)(2,1)S(1)}, bf16[2048,16]{0,1:T(8,128)(2,1)}, u32[]{:S(2)}) copy-start(bf16[2048,16]{0,1:T(8,128)(2,1)} %param.23) | copy-start | bytes 196612
  10.5 4.8 %copy-start.14 = (f32[16]{0:T(128)S(1)}, f32[16]{0:T(128)}, u32[]{:S(2)}) copy-start(f32[16]{0:T(128)} %param.24) | copy-start | bytes 196
  14.9 1.2 copy-start.15
  15.5 0.6 copy-start.9
  15.5 1.0 copy-start.5
  15.5 1.8 copy-start.11
  17.3 22.3 %copy-start.10 = (bf16[2048]{0:T(1024)(128)(2,1)S(1)}, bf16[2048]{0:T(1024)(128)(2,1)}, u32[]{:S(2)}) copy-start(bf16[2048]{0:T(1024)(128)(2,1)} %param.30) | copy-start | bytes 12292
  17.3 22.3 %copy-start.7 = (s32[16,6]{0,1:T(8,128)S(1)}, s32[16,6]{0,1:T(8,128)}, u32[]{:S(2)}) copy-start(s32[16,6]{0,1:T(8,128)} %param.31) | copy-start | bytes 1156
  17.3 84.5 %copy-start.6 = (bf16[16,2048]{1,0:T(8,128)(2,1)S(1)}, bf16[16,2048]{1,0:T(8,128)(2,1)}, u32[]{:S(2)}) copy-start(bf16[16,2048]{1,0:T(8,128)(2,1)} %param.29) | copy-start | bytes 196612
  111.4 21.8 %all-to-all-start.1 = ((bf16[128,2,128]{2,1,0:T(2,128)(2,1)}), bf16[128,2,128]{2,1,0:T(2,128)(2,1)S(1)}, u32[]{:S(2)}, u32[]{:S(2)}) async-start(bf16[128,2,128]{2,1,0:T(2,128)(2,1)} %reshape.232), calls=%async_computation.1 | async-start | bytes 131072 | tf_op jit(solution)/shard_map/all_to_all | solution.py:136
  135.9 0.7 copy-start.3
  138.9 34.3 %copy-start.12 = (bf16[1,2048,256]{2,1,0:T(8,128)(2,1)S(1)}, bf16[1,2048,256]{2,1,0:T(8,128)(2,1)}, u32[]{:S(2)}) copy-start(bf16[1,2048,256]{2,1,0:T(8,128)(2,1)} %param.33) | copy-start | bytes 3145732
  187.7 9.9 %copy-start.8 = (f32[16,6]{0,1:T(8,128)S(1)}, f32[16,6]{0,1:T(8,128)}, u32[]{:S(2)}) copy-start(f32[16,6]{0,1:T(8,128)} %param.32) | copy-start | bytes 1156
  188.8 28.3 %copy-start.4 = (f32[16,2048]{1,0:T(8,128)S(1)}, f32[16,2048]{1,0:T(8,128)}, u32[]{:S(2)}) copy-start(f32[16,2048]{1,0:T(8,128)} %copy-done.3) | copy-start | bytes 393220
  191.3 25.4 %all-to-all-start.4 = ((bf16[128,1,2,1024]{3,2,1,0:T(2,128)(2,1)}), bf16[128,1,2,1024]{3,2,1,0:T(2,128)(2,1)S(1)}, u32[]{:S(2)}, u32[]{:S(2)}) async-start(bf16[128,1,2,1024]{3,2,1,0:T(2,128)(2,1)} %copy.51), calls=%async_computation.4 | async-start | bytes 1048576 | tf_op jit(solution)/shard_map/all_to_all | solution.py:169
Sparse Core Ops, SparseCore 0:
  39.7 61.9 all-gather.1
where the time goes:
time: 229 us
  waiting for transfers between devices  91.2 us (40%)
  blocking collectives  72.8 us (32%)
  starting transfers between devices  17.3 us (8%)
  matrix products  15.3 us (7%)
  between operations  14.4 us (6%)
  local copies, waits for them, and re-layouts  10.8 us (5%)
  other arithmetic  6.73 us (3%)
    all_gather x1, waiting for transfers between devices, gather_axes(): nearer = lax.all_gather(array, axes[-1], axis=dim, tiled=True)  61.5 us
    all_to_all x1, blocking collectives, per_device(): lax.all_to_all(outgoing, EP, split_axis=0, concat_axis=0, tiled=True)  34.3 us
    all_gather x2, blocking collectives, gather_axes(): nearer = lax.all_gather(array, axes[-1], axis=dim, tiled=True)  21.4 us
    all_to_all x1, waiting for transfers between devices, per_device(): lax.all_to_all(half_sum, EP, split_axis=0, concat_axis=0, tiled=True)  19 us
    all_to_all x1, starting transfers between devices, per_device(): lax.all_to_all(projected, EP, split_axis=0, concat_axis=1, tiled=True)  11.1 us
    all_to_all x1, waiting for transfers between devices, per_device(): lax.all_to_all(projected, EP, split_axis=0, concat_axis=1, tiled=True)  10.7 us
    all_to_all x1, blocking collectives, sum_at_owner(): lax.all_to_all(blocks, axis, split_axis=0, concat_axis=0, tiled=True)  8.62 us
    all_to_all x1, starting transfers between devices, per_device(): lax.all_to_all(half_sum, EP, split_axis=0, concat_axis=0, tiled=True)  6.17 us
  transfers between devices with their start and end apart: 3, of which 3 were waited for; matrix products, arithmetic and copies ran while one was open for 0% of the time, Pallas kernels for 0%

commit v1 on v0

v1 whole, which is shorter than its diff:
```python
import jax
import jax.numpy as jnp
from jax import lax
from jax.sharding import Mesh
from jax.experimental import pallas as pl
from jax.experimental.pallas import tpu as pltpu
from jax.sharding import PartitionSpec as P

HD = 64
TOP_K = 6
EP = ("ep_0", "ep_1", "ep_2")


epsilon = 1e-06


def root_norm(values_in, gain):
    floats = values_in.astype(jnp.float32)
    inv_root = lax.rsqrt(jnp.mean(floats * floats, axis=-1, keepdims=True) + epsilon)
    return floats * inv_root * gain.astype(jnp.float32)


NZ = 8
NX = 4
PLANE = 16
ROWS = 16
HALF = 1024
MESH = pl.DeviceIdType.MESH


def layer_kernel(
    att_ref,
    hid_ref,
    wo_ref,
    gain_ref,
    info_ref,
    gate_ref,
    up_ref,
    down_ref,
    out_ref,
    hsub,
    hall,
    infoall,
    wall,
    aall,
    part,
    part_in,
    mixed,
    res,
    sq,
    sq_in,
    disp,
    xrow,
    gate_v,
    up_v,
    down_v,
    o_out,
    o_in,
    ret,
    back,
    psum,
    tsum,
    upd,
    upd_in,
    z_send,
    z_recv,
    p_send,
    p_recv,
    f_send,
    f_recv,
    t_send,
    t_recv,
    w_sem,
):
    z = lax.axis_index("ep_0")
    y = lax.axis_index("ep_1")
    x = lax.axis_index("ep_2")
    t = lax.axis_index("tp")
    me = y * NX + x
    o = 1 - t

    def z_copy(phase, src, dst, i, zz, slot):
        return pltpu.make_async_remote_copy(
            src_ref=src,
            dst_ref=dst,
            send_sem=z_send.at[phase, i],
            recv_sem=z_recv.at[phase, slot],
            device_id={"ep_0": zz},
            device_id_type=MESH,
        )

    def p_copy(phase, src, dst, i, pp, slot):
        return pltpu.make_async_remote_copy(
            src_ref=src,
            dst_ref=dst,
            send_sem=p_send.at[phase, i],
            recv_sem=p_recv.at[phase, slot],
            device_id={"ep_1": pp // NX, "ep_2": lax.rem(pp, NX)},
            device_id_type=MESH,
        )

    def t_copy(phase, src, dst):
        return pltpu.make_async_remote_copy(
            src_ref=src,
            dst_ref=dst,
            send_sem=t_send.at[phase],
            recv_sem=t_recv.at[phase],
            device_id={"tp": o},
            device_id_type=MESH,
        )

    def over_z(fn):
        def step(d, carry):
            fn(d, lax.rem(z + d, NZ))
            return carry

        lax.fori_loop(1, NZ, step, 0)

    def over_plane(fn):
        def step(d, carry):
            fn(d, lax.rem(me + d, PLANE))
            return carry

        lax.fori_loop(1, PLANE, step, 0)

    barrier = pltpu.get_barrier_semaphore()
    over_z(lambda d, zz: pl.semaphore_signal(barrier, inc=1, device_id={"ep_0": zz}, device_id_type=MESH))
    over_plane(
        lambda d, pp: pl.semaphore_signal(
            barrier,
            inc=1,
            device_id={"ep_1": pp // NX, "ep_2": lax.rem(pp, NX)},
            device_id_type=MESH,
        )
    )
    pl.semaphore_signal(barrier, inc=1, device_id={"tp": o}, device_id_type=MESH)

    loads = []
    for zz in range(NZ):
        for h in range(2):
            rows = pl.ds(zz * 256 + h * 128, 128)
            put = pl.ds(zz * 128, 128)
            n = zz * 2 + h
            loads.append(pltpu.make_async_copy(gate_ref.at[0, rows, :], gate_v.at[h, put, :], w_sem.at[0, n]))
            loads.append(pltpu.make_async_copy(up_ref.at[0, rows, :], up_v.at[h, put, :], w_sem.at[1, n]))
            loads.append(pltpu.make_async_copy(down_ref.at[0, :, rows], down_v.at[h, :, put], w_sem.at[2, n]))
    for load in loads:
        load.start()

    for zz in range(NZ):
        hsub[:, zz * 128 : (zz + 1) * 128] = hid_ref[:, pl.ds(pl.multiple_of(zz * 256 + t * 128, 128), 128)]
    hall[z] = hsub[...]
    infoall[z] = info_ref[...]
    aall[z] = att_ref[...]
    my_columns = pl.ds(pl.multiple_of(t * HALF, HALF), HALF)
    wall[me] = wo_ref[:, my_columns]

    pl.semaphore_wait(barrier, (NZ - 1) + (PLANE - 1) + 1)

    over_z(lambda d, zz: z_copy(0, att_ref, aall.at[z], d, zz, z).start())
    over_plane(lambda d, pp: p_copy(0, wo_ref.at[:, my_columns], wall.at[me], d, pp, me).start())
    over_z(lambda d, zz: z_copy(1, info_ref, infoall.at[z], d, zz, z).start())
    over_z(lambda d, zz: z_copy(2, hsub, hall.at[z], d, zz, z).start())

    over_plane(lambda d, pp: p_copy(0, wo_ref.at[:, my_columns], wall.at[pp], d, pp, pp).wait_recv())
    over_z(lambda d, zz: z_copy(0, att_ref, aall.at[zz], d, zz, zz).wait_recv())

    att = aall[...].reshape(NZ * ROWS, HALF)
    for h in range(2):
        weights = wall[h * 8 : (h + 1) * 8].reshape(128, HALF)
        part[h] = lax.dot_general(att, weights, (((1,), (1,)), ((), ())), preferred_element_type=jnp.float32)
    give = t_copy(0, part.at[o], part_in)
    give.start()

    over_z(lambda d, zz: z_copy(1, info_ref, infoall.at[zz], d, zz, zz).wait_recv())
    info = jnp.sum(infoall[...], axis=0)
    row = lax.broadcasted_iota(jnp.int32, (PLANE * ROWS, NZ * ROWS), 0)
    token = lax.broadcasted_iota(jnp.int32, (PLANE * ROWS, NZ * ROWS), 1)
    expert = (row // ROWS + z * PLANE).astype(jnp.float32)
    named = jnp.zeros((PLANE * ROWS, NZ * ROWS), jnp.float32)
    scale = jnp.zeros((PLANE * ROWS, NZ * ROWS), jnp.float32)
    for j in range(TOP_K):
        hit = info[j : j + 1, :] == expert
        named = named + jnp.where(hit, 1.0, 0.0)
        scale = scale + jnp.where(hit, info[8 + j : 9 + j, :], 0.0)
    first = lax.broadcasted_iota(jnp.int32, (NZ * ROWS, NZ * ROWS), 0)
    second = lax.broadcasted_iota(jnp.int32, (NZ * ROWS, NZ * ROWS), 1)
    ahead = jnp.where((first // ROWS == second // ROWS) & (first < second), 1.0, 0.0).astype(jnp.bfloat16)
    rank = jnp.dot(named.astype(jnp.bfloat16), ahead, preferred_element_type=jnp.float32)
    slot = lax.rem(row, 2).astype(jnp.float32)
    here = lax.rem(row, ROWS) // 2 == token // ROWS
    pick = jnp.where(here & (rank == slot), named, 0.0)
    pick_half = pick.astype(jnp.bfloat16)
    combine = jnp.transpose(pick * scale)
    combine_high = combine.astype(jnp.bfloat16)
    combine_low = (combine - combine_high.astype(jnp.float32)).astype(jnp.bfloat16)

    give.wait_recv()
    mixed[z] = (part[t] + part_in[...]).astype(jnp.bfloat16)
    over_z(lambda d, zz: z_copy(3, mixed.at[z], mixed.at[z], d, zz, z).start())
    over_z(lambda d, zz: z_copy(2, hsub, hall.at[zz], d, zz, zz).wait_recv())
    over_z(lambda d, zz: z_copy(3, mixed.at[zz], mixed.at[zz], d, zz, zz).wait_recv())

    squares = jnp.zeros((NZ * ROWS, 128), jnp.float32)
    for zz in range(NZ):
        block = hall[:, :, zz * 128 : (zz + 1) * 128].reshape(NZ * ROWS, 128).astype(jnp.float32)
        block = block + mixed[zz].astype(jnp.float32)
        res[zz] = block
        squares = squares + block * block
    sq[...] = jnp.broadcast_to(jnp.sum(squares, axis=-1, keepdims=True), (NZ * ROWS, 128))
    give_sq = t_copy(1, sq, sq_in)
    give_sq.start()
    give_sq.wait_recv()
    inverse = lax.rsqrt((sq[...] + sq_in[...]) * (1.0 / 2048.0) + epsilon)
    for zz in range(NZ):
        gain = gain_ref[pl.ds(2 * zz + t, 1), :]
        block = (res[zz] * inverse * gain).astype(jnp.bfloat16)
        rows = jnp.dot(pick_half, block, preferred_element_type=jnp.float32)
        disp[:, :, zz * 128 : (zz + 1) * 128] = rows.astype(jnp.bfloat16).reshape(PLANE, ROWS, 128)

    over_plane(lambda d, pp: p_copy(1, disp.at[pp], xrow.at[t, me], d, pp, me).start())
    xrow[t, me] = disp[me]

    def forward(pp):
        return pltpu.make_async_remote_copy(
            src_ref=xrow.at[t, pp],
            dst_ref=xrow.at[t, pp],
            send_sem=f_send.at[pp],
            recv_sem=f_recv.at[pp],
            device_id={"tp": o},
            device_id_type=MESH,
        )

    def arrival(pp):
        return pltpu.make_async_remote_copy(
            src_ref=xrow.at[o, pp],
            dst_ref=xrow.at[o, pp],
            send_sem=f_send.at[pp],
            recv_sem=f_recv.at[pp],
            device_id={"tp": o},
            device_id_type=MESH,
        )

    forward(me).start()

    def pass_on(d, pp):
        p_copy(1, disp.at[pp], xrow.at[t, pp], d, pp, pp).wait_recv()
        forward(pp).start()

    over_plane(pass_on)
    for load in loads:
        load.wait()
    mine = xrow[t].reshape(PLANE * ROWS, HALF)
    gate_act = jnp.dot(mine, gate_v[t], preferred_element_type=jnp.float32)
    up_act = jnp.dot(mine, up_v[t], preferred_element_type=jnp.float32)
    over = lax.fori_loop(0, PLANE, lambda i, c: (arrival(i).wait_recv(), c)[1], 0)
    other = xrow[o].reshape(PLANE * ROWS, HALF)
    gate_act = gate_act + jnp.dot(other, gate_v[o], preferred_element_type=jnp.float32)
    up_act = up_act + jnp.dot(other, up_v[o], preferred_element_type=jnp.float32)
    act = (gate_act * (1.0 / (1.0 + jnp.exp(-gate_act))) * up_act).astype(jnp.bfloat16)
    o_out[...] = jnp.dot(act, down_v[o], preferred_element_type=jnp.float32).astype(jnp.bfloat16)
    give_o = t_copy(2, o_out, o_in)
    give_o.start()
    own = jnp.dot(act, down_v[t], preferred_element_type=jnp.float32).astype(jnp.bfloat16)
    give_o.wait_recv()
    both = own.astype(jnp.float32) + o_in[...].astype(jnp.float32)
    ret[...] = both.astype(jnp.bfloat16).reshape(PLANE, ROWS, HALF)
    over_plane(lambda d, pp: p_copy(2, ret.at[pp], back.at[me], d, pp, me).start())
    back[me] = ret[me]
    over_plane(lambda d, pp: p_copy(2, ret.at[pp], back.at[pp], d, pp, pp).wait_recv())

    outs = back[...].reshape(PLANE * ROWS, HALF)
    total = jnp.dot(combine_high, outs, preferred_element_type=jnp.float32)
    total = total + jnp.dot(combine_low, outs, preferred_element_type=jnp.float32)
    psum[...] = total.astype(jnp.bfloat16).reshape(NZ, ROWS, HALF)
    over_z(lambda d, zz: z_copy(4, psum.at[zz], tsum.at[z], d, zz, z).start())
    tsum[z] = psum[z]
    over_z(lambda d, zz: z_copy(4, psum.at[zz], tsum.at[zz], d, zz, zz).wait_recv())
    mix = jnp.sum(tsum[...].astype(jnp.float32), axis=0)
    my_rows = pl.ds(pl.multiple_of(z * ROWS, ROWS), ROWS)
    for zz in range(NZ):
        upd[:, zz * 128 : (zz + 1) * 128] = (
            res[zz, my_rows, :] + mix[:, zz * 128 : (zz + 1) * 128]
        ).astype(jnp.bfloat16)
    give_u = t_copy(3, upd, upd_in)
    give_u.start()
    for zz in range(NZ):
        out_ref[:, pl.ds(pl.multiple_of(zz * 256 + t * 128, 128), 128)] = upd[:, zz * 128 : (zz + 1) * 128]
    give_u.wait_recv()
    for zz in range(NZ):
        out_ref[:, pl.ds(pl.multiple_of(zz * 256 + o * 128, 128), 128)] = upd_in[:, zz * 128 : (zz + 1) * 128]

    over_z(lambda d, zz: z_copy(0, att_ref, aall.at[z], d, zz, z).wait_send())
    over_z(lambda d, zz: z_copy(1, info_ref, infoall.at[z], d, zz, z).wait_send())
    over_z(lambda d, zz: z_copy(2, hsub, hall.at[z], d, zz, z).wait_send())
    over_z(lambda d, zz: z_copy(3, mixed.at[z], mixed.at[z], d, zz, z).wait_send())
    over_z(lambda d, zz: z_copy(4, psum.at[zz], tsum.at[z], d, zz, z).wait_send())
    over_plane(lambda d, pp: p_copy(0, wo_ref.at[:, my_columns], wall.at[me], d, pp, me).wait_send())
    over_plane(lambda d, pp: p_copy(1, disp.at[pp], xrow.at[t, me], d, pp, me).wait_send())
    over_plane(lambda d, pp: p_copy(2, ret.at[pp], back.at[me], d, pp, me).wait_send())
    lax.fori_loop(0, PLANE, lambda i, c: (forward(i).wait_send(), c)[1], 0)
    for give_one in (give, give_sq, give_o, give_u):
        give_one.wait_send()


def after_attention(attended, hidden, out_weight, ffn_gain, info, gate_weights, up_weights, down_weights):
    bf16, f32 = jnp.bfloat16, jnp.float32
    tokens = NZ * ROWS
    vmem = pl.BlockSpec(memory_space=pltpu.VMEM)
    hbm = pl.BlockSpec(memory_space=pl.ANY)
    return pl.pallas_call(
        layer_kernel,
        out_shape=jax.ShapeDtypeStruct(hidden.shape, bf16),
        in_specs=[vmem] * 5 + [hbm] * 3,
        out_specs=vmem,
        scratch_shapes=[
            pltpu.VMEM((ROWS, HALF), bf16),
            pltpu.VMEM((NZ, ROWS, HALF), bf16),
            pltpu.VMEM((NZ, 16, 128), f32),
            pltpu.VMEM((PLANE, ROWS, HALF), bf16),
            pltpu.VMEM((NZ, ROWS, HALF), bf16),
            pltpu.VMEM((2, tokens, 128), f32),
            pltpu.VMEM((tokens, 128), f32),
            pltpu.VMEM((NZ, tokens, 128), bf16),
            pltpu.VMEM((NZ, tokens, 128), f32),
            pltpu.VMEM((tokens, 128), f32),
            pltpu.VMEM((tokens, 128), f32),
            pltpu.VMEM((PLANE, ROWS, HALF), bf16),
            pltpu.VMEM((2, PLANE, ROWS, HALF), bf16),
            pltpu.VMEM((2, HALF, 256), bf16),
            pltpu.VMEM((2, HALF, 256), bf16),
            pltpu.VMEM((2, 256, HALF), bf16),
            pltpu.VMEM((PLANE * ROWS, HALF), bf16),
            pltpu.VMEM((PLANE * ROWS, HALF), bf16),
            pltpu.VMEM((PLANE, ROWS, HALF), bf16),
            pltpu.VMEM((PLANE, ROWS, HALF), bf16),
            pltpu.VMEM((NZ, ROWS, HALF), bf16),
            pltpu.VMEM((NZ, ROWS, HALF), bf16),
            pltpu.VMEM((ROWS, HALF), bf16),
            pltpu.VMEM((ROWS, HALF), bf16),
            pltpu.SemaphoreType.DMA((5, NZ)),
            pltpu.SemaphoreType.DMA((5, NZ)),
            pltpu.SemaphoreType.DMA((3, PLANE)),
            pltpu.SemaphoreType.DMA((3, PLANE)),
            pltpu.SemaphoreType.DMA((PLANE,)),
            pltpu.SemaphoreType.DMA((PLANE,)),
            pltpu.SemaphoreType.DMA((4,)),
            pltpu.SemaphoreType.DMA((4,)),
            pltpu.SemaphoreType.DMA((3, 16)),
        ],
        compiler_params=pltpu.CompilerParams(
            collective_id=0, has_side_effects=True, vmem_limit_bytes=56 * 1024 * 1024
        ),
    )(attended, hidden, out_weight, ffn_gain, info, gate_weights, up_weights, down_weights)


def per_device(
    hidden,
    attn_gain,
    query_weight,
    key_weight,
    value_weight,
    forget_weight,
    forget_bias,
    cache_keys,
    cache_values,
    cache_logsum,
    lengths,
    out_weight,
    ffn_gain,
    expert_ids,
    expert_scores,
    gate_weights,
    up_weights,
    down_weights,
):
    rows_here = hidden.shape[0]
    query_heads = query_weight.shape[1] // HD
    key_heads = key_weight.shape[1] // HD
    group_size = query_heads // key_heads
    cache_len = cache_keys.shape[-1]
    score_scale = HD ** (-0.5)
    normed = root_norm(hidden, attn_gain).astype(jnp.bfloat16)
    queries = jnp.dot(normed, query_weight, preferred_element_type=jnp.float32).astype(jnp.bfloat16)
    key_new = (
        jnp.dot(normed, key_weight, preferred_element_type=jnp.float32)
        .astype(jnp.bfloat16)
        .reshape(rows_here, key_heads, HD)
    )
    value_new = (
        jnp.dot(normed, value_weight, preferred_element_type=jnp.float32)
        .astype(jnp.bfloat16)
        .reshape(rows_here, key_heads, HD)
    )
    log_forget = jax.nn.log_sigmoid(
        jnp.dot(normed, forget_weight, preferred_element_type=jnp.float32) + forget_bias
    )
    positions = jnp.arange(cache_len, dtype=jnp.int32)
    is_last = positions[None, :] == (lengths - 1)[:, None]
    new_logsum = jnp.sum(jnp.where(is_last[:, None, :], cache_logsum, 0.0), axis=-1) + log_forget
    grouped = queries.reshape(rows_here, key_heads, group_size, HD)
    scores = jnp.einsum("sgjd,sgdp->sgjp", grouped, cache_keys, preferred_element_type=jnp.float32)
    scores = scores.reshape(rows_here, query_heads, cache_len) * score_scale
    scores = scores + new_logsum[:, :, None] - cache_logsum
    is_live = positions[None, :] < lengths[:, None]
    scores = jnp.where(is_live[:, None, :], scores, -jnp.inf)
    own_score = (
        jnp.einsum("sgjd,sgd->sgj", grouped, key_new, preferred_element_type=jnp.float32).reshape(
            rows_here, query_heads
        )
        * score_scale
    )
    top_score = jnp.maximum(jnp.max(scores, axis=-1), own_score)
    past_exp = jnp.exp(scores - top_score[:, :, None])
    own_exp = jnp.exp(own_score - top_score)
    denominator = jnp.sum(past_exp, axis=-1) + own_exp
    past_weight = (past_exp / denominator[:, :, None]).astype(jnp.bfloat16)
    own_weight = (own_exp / denominator).astype(jnp.bfloat16)
    attended = jnp.einsum(
        "sgjp,sgdp->sgjd",
        past_weight.reshape(rows_here, key_heads, group_size, cache_len),
        cache_values,
        preferred_element_type=jnp.float32,
    )
    attended = (
        attended
        + own_weight.astype(jnp.float32).reshape(rows_here, key_heads, group_size)[:, :, :, None]
        * value_new.astype(jnp.float32)[:, :, None, :]
    )
    attended = attended.reshape(rows_here, query_heads * HD).astype(jnp.bfloat16)
    route_weight = expert_scores / jnp.sum(expert_scores, axis=-1, keepdims=True)
    facts = jnp.zeros((16, rows_here), jnp.float32)
    facts = facts.at[:TOP_K].set(expert_ids.astype(jnp.float32).T).at[8 : 8 + TOP_K].set(route_weight.T)
    lanes = jnp.arange(NZ * ROWS, dtype=jnp.int32) // ROWS
    info = jnp.where(lanes[None, :] == lax.axis_index("ep_0"), jnp.tile(facts, (1, NZ)), 0.0)
    gain = ffn_gain.astype(jnp.float32).reshape(16, 128)
    updated = after_attention(
        attended, hidden, out_weight, gain, info, gate_weights, up_weights, down_weights
    )
    return (updated, key_new, value_new, new_logsum)


def solution(mesh):
    split = Mesh(mesh.devices.reshape(8, 4, 4, mesh.shape["tp"]), ("ep_0", "ep_1", "ep_2", "tp"))
    in_specs = (
        P(EP, None),
        P(),
        P(None, "tp"),
        P(None, "tp"),
        P(None, "tp"),
        P(None, "tp"),
        P("tp"),
        P(EP, "tp", None, None),
        P(EP, "tp", None, None),
        P(EP, "tp", None),
        P(EP),
        P(EP, None),
        P(),
        P(EP, None),
        P(EP, None),
        P(EP, None, "tp"),
        P(EP, None, "tp"),
        P(EP, "tp", None),
    )
    out_specs = (P(EP, None), P(EP, "tp", None), P(EP, "tp", None), P(EP, "tp"))
    return jax.shard_map(
        per_device, mesh=split, in_specs=in_specs, out_specs=out_specs, check_vma=False
    )
```

time: 229 us -> 83.8 us (0.37)
  waiting for transfers between devices: 91.2 us -> 0 us
  blocking collectives: 72.8 us -> 0 us
  Pallas kernels: 0 us -> 70.2 us
  starting transfers between devices: 17.3 us -> 0 us
  between operations: 14.4 us -> 0.87 us
  matrix products: 15.3 us -> 5.67 us
  local copies, waits for them, and re-layouts: 10.8 us -> 3.03 us
  other arithmetic: 6.73 us -> 3.74 us
    pallas_call x0 -> x1, Pallas kernels: none -> 70.2 us  [after_attention(): pl.pallas_call(layer_kernel, out_shape=jax.ShapeDtypeStruct(hidden.shape,...]
    all_gather x1 -> x0, waiting for transfers between devices: 61.5 us -> none  [gather_axes(): nearer = lax.all_gather(array, axes[-1], axis=dim, tiled=True)]
    all_to_all x3 -> x0, blocking collectives: 47.4 us -> none  [the longest x1 34.3 us: per_device(): lax.all_to_all(outgoing, EP, split_axis=0, concat_axis=0, tiled=True)]
    all_to_all x2 -> x0, waiting for transfers between devices: 29.6 us -> none  [the longest x1 19 us: per_device(): lax.all_to_all(half_sum, EP, split_axis=0, concat_axis=0, tiled=True)]
    all_gather x3 -> x0, blocking collectives: 25.4 us -> none  [the longest x2 21.4 us: gather_axes(): nearer = lax.all_gather(array, axes[-1], axis=dim, tiled=True)]
    all_to_all x2 -> x0, starting transfers between devices: 17.3 us -> none  [the longest x1 11.1 us: per_device(): lax.all_to_all(projected, EP, split_axis=0, concat_axis=1, tiled=True)]
    dot_general x5 -> x0, matrix products: 8.71 us -> none  [the longest x1 3.82 us: per_device(): jnp.einsum('sekf,efd->sekd', hidden_act, down_weights, preferred_element_...]
    reshape x5 -> x0, local copies, waits for them, and re-layouts: 3.27 us -> none  [the longest x1 1.52 us: per_device(): outgoing.astype(jnp.bfloat16)]
  transfers between devices with their start and end apart: 3 -> 0, of which waited for: 3 -> 0; matrix products, arithmetic and copies ran while one was open for 0% -> 0% of each run, Pallas kernels for 0% -> 0%
where the time goes in v1:
time: 83.8 us; the launch traced here: 83.5 us
  Pallas kernels  70.2 us (84%)
  matrix products  5.67 us (7%)
  other arithmetic  3.74 us (4%)
  local copies, waits for them, and re-layouts  3.03 us (4%)
  between operations  0.87 us (1%)
    pallas_call x1, Pallas kernels, after_attention(): pl.pallas_call(layer_kernel, out_shape=jax.ShapeDtypeStruct(hidden.shape,...  70.2 us
    dot_general x1, matrix products, per_device(): jnp.dot(normed, query_weight, preferred_element_type=jnp.float32)  3.01 us
    unnamed x29, local copies, waits for them, and re-layouts  1.95 us

profile of v1, /device:TPU:1, one launch (start us, length us, event | category | flops | bytes accessed | tf_op | source)
XLA Modules:
  0.0 83.5 jit_solution(12550030504206796356)
XLA Ops:
  0.6 0.0 copy-start
  0.6 0.8 %convert_element_type.45 = f32[2048]{0:T(1024)S(1)} convert(bf16[2048]{0:T(1024)(128)(2,1)} %param.23) | non-fusion elementwise | flops 2048 | bytes 12288 | tf_op jit(solution)/shard_map/convert_element_type | solution.py:20
  1.5 1.0 %fusion.26 = f32[16]{0:T(128)S(1)} fusion(bf16[16,2048]{1,0:T(8,128)(2,1)} %hid_ref.1), kind=kLoop, calls=%fused_computation.23 | loop fusion | flops 98288 | bytes 65600 | tf_op jit(solution)/shard_map/reduce_sum | solution.py:19
  2.5 0.0 copy-start.8
  2.5 0.0 copy-start.1
  2.5 0.0 copy-start.2
  2.5 0.0 copy-start.11
  2.5 0.0 copy-start.12
  2.5 3.0 %convolution_convert_fusion = bf16[16,1024]{1,0:T(8,128)(2,1)S(1)} fusion(bf16[2048,1024]{1,0:T(8,128)(2,1)} %param.24, bf16[16,2048]{1,0:T(8,128)(2,1)} %hid_ref.1, f32[2048]{0:T(1024)S(1)} %convert_element_type.45, f32[16]{0:T(128)S(1)} %add_rsqrt_fusion), kind=kOutput, calls=%fused_computation.10 | convolution fusion | flops 67256320 | bytes 4300864 | tf_op jit(solution)/shard_map/dot_general | solution.py:384
  5.5 0.1 reshape.202
  5.6 0.0 copy-done.8
  5.7 0.1 iota_compare_fusion
  5.8 0.0 copy-done.1
  5.8 0.2 select_reduce_fusion
  5.9 0.0 copy-done.2
  6.0 0.0 copy-done.11
  6.0 0.0 copy-done.12
  6.0 0.2 fusion.30
  6.2 0.0 copy-start.5
  6.2 0.1 iota_compare_fusion.1
  6.3 0.0 copy-done
  6.3 0.0 copy-start.10
  6.3 0.0 copy-start.3
  6.3 0.0 copy-start.9
  6.4 0.5 fusion.40
  6.9 0.0 copy-done.5
  6.9 0.4 copy-done.10
  7.3 0.2 convolution_convert_fusion.2
  7.5 0.0 copy-start.13
  7.5 0.1 fusion.31
  7.7 0.3 fusion.23
  8.0 0.0 copy-done.3
  8.0 0.8 %fusion.41 = (f32[16,64]{1,0:T(8,128)S(1)}, bf16[16,64]{1,0:T(8,128)(2,1)}) fusion(bf16[2048,64]{0,1:T(8,128)(2,1)S(1)} %copy-done.3, bf16[16,2048]{1,0:T(8,128)(2,1)S(1)} %copy-done.2, f32[2048]{0:T(1024)S(1)} %convert_element_type.45, f32[16]{0:T(128)S(1)} %add_rsqrt_fusion), kind=kOutput, calls=%fused_computation.50 | convolution fusion | flops 4327424 | bytes 342080 | tf_op jit(solution)/shard_map/dot_general | solution.py:391
  8.9 0.0 copy-done.9
  8.9 0.0 copy-start.7
  8.9 0.0 copy-start.4
  8.9 0.0 copy-start.6
  8.9 0.7 fusion.19
  9.6 0.0 copy-done.13
  9.6 0.7 convert_element_type.55.att_ref
  10.3 0.0 copy-done.7
  10.3 0.0 copy-done.4
  10.4 0.1 scatter.9
  10.5 0.1 tile.13
  10.6 0.6 broadcast_select_fusion.info_ref
  11.2 0.0 copy-done.6
  11.2 0.6 bitcast_convert_fusion.gain_ref
  11.8 70.2 %shard_map.201 = bf16[16,2048]{1,0:T(8,128)(2,1)} custom-call(bf16[16,1024]{1,0:T(8,128)(2,1)} %convert_element_type.55.att_ref, bf16[16,2048]{1,0:T(8,128)(2,1)} %hid_ref.1, bf16[16,2048]{1,0:T(8,128)(2,1)} %wo_ref.1, f32[16,128]{1,0:T(8,128)} %bitcast_convert_fusion.gain_ref, f32[16,128]{1,0:T(8,128)} %broadcast_select_fusion.info_ref, ...), custom_call_target="tpu_custom_call" | custom-call | tf_op jit(solution)/shard_map/pallas_call | solution.py:311
  82.1 1.5 %copy.28 = bf16[16,2048]{1,0:T(8,128)(2,1)} copy(bf16[16,2048]{1,0:T(8,128)(2,1)} %shard_map.201) | data formatting | bytes 131072
  (10 shorter events, 0.1 us)
Async XLA Ops:
  0.6 5.7 %copy-start = (bf16[16,1,64,1024]{3,2,1,0:T(8,128)(2,1)S(1)}, bf16[16,1,64,1024]{3,2,1,0:T(8,128)(2,1)}, u32[]{:S(2)}) copy-start(bf16[16,1,64,1024]{3,2,1,0:T(8,128)(2,1)} %param.29) | copy-start | bytes 6291460
  2.5 3.2 %copy-start.8 = (s32[16]{0:T(128)S(1)}, s32[16]{0:T(128)}, u32[]{:S(2)}) copy-start(s32[16]{0:T(128)} %param.32) | copy-start | bytes 196
  2.5 3.3 %copy-start.1 = (f32[16,16,1024]{2,1,0:T(8,128)S(1)}, f32[16,16,1024]{2,1,0:T(8,128)}, u32[]{:S(2)}) copy-start(f32[16,16,1024]{2,1,0:T(8,128)} %param.31) | copy-start | bytes 3145732
  2.5 3.5 %copy-start.2 = (bf16[16,2048]{1,0:T(8,128)(2,1)S(1)}, bf16[16,2048]{1,0:T(8,128)(2,1)}, u32[]{:S(2)}) copy-start(bf16[16,2048]{1,0:T(8,128)(2,1)} %hid_ref.1) | copy-start | bytes 196612
  2.5 3.5 %copy-start.11 = (bf16[2048,16]{0,1:T(8,128)(2,1)S(1)}, bf16[2048,16]{0,1:T(8,128)(2,1)}, u32[]{:S(2)}) copy-start(bf16[2048,16]{0,1:T(8,128)(2,1)} %param.27) | copy-start | bytes 196612
  2.5 3.5 %copy-start.12 = (f32[16]{0:T(128)S(1)}, f32[16]{0:T(128)}, u32[]{:S(2)}) copy-start(f32[16]{0:T(128)} %param.28) | copy-start | bytes 196
  6.2 0.7 copy-start.5
  6.3 1.0 %copy-start.10 = (bf16[2048,64]{0,1:T(8,128)(2,1)S(1)}, bf16[2048,64]{0,1:T(8,128)(2,1)}, u32[]{:S(2)}) copy-start(bf16[2048,64]{0,1:T(8,128)(2,1)} %param.25) | copy-start | bytes 786436
  6.3 1.7 %copy-start.3 = (bf16[2048,64]{0,1:T(8,128)(2,1)S(1)}, bf16[2048,64]{0,1:T(8,128)(2,1)}, u32[]{:S(2)}) copy-start(bf16[2048,64]{0,1:T(8,128)(2,1)} %param.26) | copy-start | bytes 786436
  6.3 2.5 %copy-start.9 = (bf16[16,1,64,1024]{3,2,1,0:T(8,128)(2,1)S(1)}, bf16[16,1,64,1024]{3,2,1,0:T(8,128)(2,1)}, u32[]{:S(2)}) copy-start(bf16[16,1,64,1024]{3,2,1,0:T(8,128)(2,1)} %param.30) | copy-start | bytes 6291460
  7.5 2.1 %copy-start.13 = (bf16[16,64]{1,0:T(8,128)(2,1)}, bf16[16,64]{1,0:T(8,128)(2,1)S(1)}, u32[]{:S(2)}) copy-start(bf16[16,64]{1,0:T(8,128)(2,1)S(1)} %convolution_convert_fusion.2) | copy-start | bytes 6148
  8.9 1.5 %copy-start.7 = (s32[16,6]{0,1:T(8,128)S(1)}, s32[16,6]{0,1:T(8,128)}, u32[]{:S(2)}) copy-start(s32[16,6]{0,1:T(8,128)} %param.35) | copy-start | bytes 1156
  8.9 1.5 %copy-start.4 = (f32[16,6]{0,1:T(8,128)S(1)}, f32[16,6]{0,1:T(8,128)}, u32[]{:S(2)}) copy-start(f32[16,6]{0,1:T(8,128)} %param.36) | copy-start | bytes 1156
  8.9 2.4 %copy-start.6 = (bf16[2048]{0:T(1024)(128)(2,1)S(1)}, bf16[2048]{0:T(1024)(128)(2,1)}, u32[]{:S(2)}) copy-start(bf16[2048]{0:T(1024)(128)(2,1)} %param.34) | copy-start | bytes 12292

commit v2 on v1

v2 whole, which is shorter than its diff:
```python
import jax
import jax.numpy as jnp
from jax import lax
from jax.experimental import pallas as pl
from jax.experimental.pallas import tpu as pltpu
from jax.sharding import Mesh
from jax.sharding import PartitionSpec as P

HD = 64
TOP_K = 6
EP = ("ep_0", "ep_1", "ep_2")
NZ = 8
NX = 4
PLANE = 16
ROWS = 16
HALF = 1024
WIDE = 2048
MESH = pl.DeviceIdType.MESH

epsilon = 1e-06


def layer_kernel(
    len_ref,
    attn_gain_ref,
    ffn_gain_ref,
    bias_ref,
    ids_ref,
    scores_ref,
    hid_hbm,
    wq_hbm,
    wk_hbm,
    wv_hbm,
    wf_hbm,
    keys_hbm,
    values_hbm,
    logsum_hbm,
    wo_ref,
    gate_ref,
    up_ref,
    down_ref,
    out_ref,
    key_out,
    value_out,
    logsum_out,
    hid_ref,
    wq,
    wkvf,
    keys,
    values,
    logsum,
    normed,
    queries,
    spread,
    heads_q,
    gate_col,
    own_col,
    new_val,
    att_rows,
    att_flat,
    att_ref,
    gains,
    info_ref,
    infoall,
    wall,
    aall,
    hcol,
    part,
    part_in,
    mixed,
    rounded,
    mown,
    rall,
    sq,
    sq_in,
    disp,
    xrow,
    gate_v,
    up_v,
    down_v,
    o_out,
    o_in,
    ret,
    back,
    psum,
    tsum,
    upd,
    upd_in,
    z_send,
    z_recv,
    p_send,
    p_recv,
    f_send,
    f_recv,
    t_send,
    t_recv,
    w_sem,
    a_sem,
):
    z = lax.axis_index("ep_0")
    y = lax.axis_index("ep_1")
    x = lax.axis_index("ep_2")
    t = lax.axis_index("tp")
    me = y * NX + x
    o = 1 - t
    parity = lax.rem(z, 2)
    pair = z // 2

    def z_copy(phase, src, dst, zz, i, slot):
        return pltpu.make_async_remote_copy(
            src_ref=src,
            dst_ref=dst,
            send_sem=z_send.at[phase, i],
            recv_sem=z_recv.at[phase, slot],
            device_id={"ep_0": zz},
            device_id_type=MESH,
        )

    def p_copy(phase, src, dst, pp, i, slot):
        return pltpu.make_async_remote_copy(
            src_ref=src,
            dst_ref=dst,
            send_sem=p_send.at[phase, i],
            recv_sem=p_recv.at[phase, slot],
            device_id={"ep_1": pp // NX, "ep_2": lax.rem(pp, NX)},
            device_id_type=MESH,
        )

    def t_copy(phase, src, dst):
        return pltpu.make_async_remote_copy(
            src_ref=src,
            dst_ref=dst,
            send_sem=t_send.at[phase],
            recv_sem=t_recv.at[phase],
            device_id={"tp": o},
            device_id_type=MESH,
        )

    def over_z(fn):
        def step(d, carry):
            fn(d, lax.rem(z + d, NZ))
            return carry

        lax.fori_loop(1, NZ, step, 0)

    def over_plane(fn):
        def step(d, carry):
            fn(d, lax.rem(me + d, PLANE))
            return carry

        lax.fori_loop(1, PLANE, step, 0)

    get_hid = pltpu.make_async_copy(hid_hbm, hid_ref, a_sem.at[0])
    get_hid.start()
    get_q = []
    for i in range(4):
        rows = pl.ds(i * 512, 512)
        get_q.append(pltpu.make_async_copy(wq_hbm.at[rows, :], wq.at[rows, :], a_sem.at[1 + i]))
    get_small = [
        pltpu.make_async_copy(wk_hbm, wkvf.at[pl.ds(0, 64)], a_sem.at[5]),
        pltpu.make_async_copy(wv_hbm, wkvf.at[pl.ds(64, 64)], a_sem.at[6]),
        pltpu.make_async_copy(wf_hbm, wkvf.at[pl.ds(128, 16)], a_sem.at[7]),
    ]
    get_cache = []
    for i in range(4):
        rows = pl.ds(i * 4, 4)
        get_cache.append(
            (
                pltpu.make_async_copy(keys_hbm.at[rows, 0], keys.at[rows], a_sem.at[8 + i]),
                pltpu.make_async_copy(logsum_hbm.at[rows], logsum.at[rows], a_sem.at[12 + i]),
                pltpu.make_async_copy(values_hbm.at[rows, 0], values.at[rows], a_sem.at[16 + i]),
            )
        )
    for copy in get_q + get_small:
        copy.start()
    for group in get_cache:
        for copy in group:
            copy.start()

    barrier = pltpu.get_barrier_semaphore()
    over_z(lambda d, zz: pl.semaphore_signal(barrier, inc=1, device_id={"ep_0": zz}, device_id_type=MESH))
    over_plane(
        lambda d, pp: pl.semaphore_signal(
            barrier,
            inc=1,
            device_id={"ep_1": pp // NX, "ep_2": lax.rem(pp, NX)},
            device_id_type=MESH,
        )
    )
    pl.semaphore_signal(barrier, inc=1, device_id={"tp": o}, device_id_type=MESH)

    info_ref[...] = jnp.zeros((2, 16, 128), jnp.float32)
    shares = scores_ref[...] / jnp.sum(scores_ref[...], axis=0, keepdims=True)
    info_ref[0, 0:TOP_K, 0:ROWS] = ids_ref[...].astype(jnp.float32)
    info_ref[0, 8 : 8 + TOP_K, 0:ROWS] = shares
    facts = info_ref[0]
    info_ref[0] = pltpu.roll(facts, pair * ROWS + parity * 64, 1)
    info_ref[1] = pltpu.roll(facts, pair * ROWS + (1 - parity) * 64, 1)
    infoall[z] = info_ref[parity]
    gains[0] = attn_gain_ref[...].astype(jnp.float32).reshape(16, 128)
    gains[1] = ffn_gain_ref[...].astype(jnp.float32).reshape(16, 128)

    get_hid.wait()
    total_sq = jnp.zeros((ROWS, 128), jnp.float32)
    for i in range(16):
        block = hid_ref[:, i * 128 : (i + 1) * 128].astype(jnp.float32)
        total_sq = total_sq + block * block
    inverse = lax.rsqrt(jnp.sum(total_sq, axis=-1, keepdims=True) * (1.0 / WIDE) + epsilon)
    for i in range(16):
        block = hid_ref[:, i * 128 : (i + 1) * 128].astype(jnp.float32)
        normed[:, i * 128 : (i + 1) * 128] = (block * inverse * gains[0, i : i + 1, :]).astype(jnp.bfloat16)
    my_columns = pl.ds(pl.multiple_of(t * HALF, HALF), HALF)

    def hid_block(zz):
        return hid_ref.at[:, pl.ds(pl.multiple_of(zz * 256 + t * 128, 128), 128)]

    hcol[0, pair] = hid_block(z)[...]

    query = jnp.zeros((ROWS, HALF), jnp.float32)
    for i in range(4):
        get_q[i].wait()
        query = query + jnp.dot(
            normed[:, i * 512 : (i + 1) * 512],
            wq[i * 512 : (i + 1) * 512, :],
            preferred_element_type=jnp.float32,
        )
    queries[...] = query.astype(jnp.bfloat16).astype(jnp.float32)

    with jax.named_scope("a_barrier"):
        pl.semaphore_wait(barrier, (NZ - 1) + (PLANE - 1) + 1)
    get_wo = pltpu.make_async_copy(wo_ref.at[:, my_columns], wall.at[me], a_sem.at[20])
    get_wo.start()

    def send_wo(d, pp):
        return p_copy(0, wo_ref.at[:, my_columns], wall.at[me], pp, d, me)

    def send_hid(d, zz):
        return z_copy(2, hid_block(zz), hcol.at[lax.rem(d, 2), pair], zz, d, z)

    def send_info(d, zz):
        return z_copy(3, info_ref.at[lax.rem(zz, 2)], infoall.at[z], zz, d, z)

    over_plane(lambda d, pp: send_wo(d, pp).start())
    over_z(lambda d, zz: send_hid(d, zz).start())
    over_z(lambda d, zz: send_info(d, zz).start())
    loads = []
    for zz in range(NZ):
        for h in range(2):
            rows = pl.ds(zz * 256 + h * 128, 128)
            put = pl.ds(zz * 128, 128)
            n = zz * 2 + h
            loads.append(pltpu.make_async_copy(gate_ref.at[0, rows, :], gate_v.at[h, put, :], w_sem.at[0, n]))
            loads.append(pltpu.make_async_copy(up_ref.at[0, rows, :], up_v.at[h, put, :], w_sem.at[1, n]))
            loads.append(pltpu.make_async_copy(down_ref.at[0, :, rows], down_v.at[h, :, put], w_sem.at[2, n]))
    for load in loads:
        load.start()

    for copy in get_small:
        copy.wait()
    three = lax.dot_general(
        normed[...], wkvf[...], (((1,), (1,)), ((), ())), preferred_element_type=jnp.float32
    )
    new_key = three[:, 0:64].astype(jnp.bfloat16)
    new_value = three[:, 64:128].astype(jnp.bfloat16)
    key_out[...] = new_key
    value_out[...] = new_value
    own_col[...] = new_key.astype(jnp.float32)
    new_val[...] = new_value.astype(jnp.float32)
    pre = three[:, 128:144] + bias_ref[...].reshape(1, 16)
    gate_col[...] = -(jnp.maximum(-pre, 0.0) + jnp.log1p(jnp.exp(-jnp.abs(pre))))

    head_of_row = lax.broadcasted_iota(jnp.int32, (ROWS, HALF), 0)
    head_of_lane = lax.broadcasted_iota(jnp.int32, (ROWS, HALF), 1) // HD
    own_lanes = head_of_row == head_of_lane
    for s in range(ROWS):
        spread[s * 16 : (s + 1) * 16, :] = jnp.where(
            own_lanes, jnp.broadcast_to(queries[s : s + 1, :], (16, HALF)), 0.0
        ).astype(jnp.bfloat16)
    fold = jnp.where(
        lax.rem(lax.broadcasted_iota(jnp.int32, (HALF, HD), 0), HD)
        == lax.broadcasted_iota(jnp.int32, (HALF, HD), 1),
        1.0,
        0.0,
    ).astype(jnp.bfloat16)
    heads_q[...] = jnp.dot(spread[...], fold, preferred_element_type=jnp.float32).astype(jnp.bfloat16)

    position = lax.broadcasted_iota(jnp.int32, (16, 1024), 1)
    diagonal = lax.broadcasted_iota(jnp.int32, (16, 16), 0) == lax.broadcasted_iota(jnp.int32, (16, 16), 1)
    score_scale = HD ** (-0.5)

    def send_att(piece, d, zz):
        rows = pl.ds(piece * 8, 8)
        return z_copy(piece, att_ref.at[rows], aall.at[lax.rem(d, 2), pair, rows], zz, d, z)

    for s in range(ROWS):
        if s % 4 == 0:
            for copy in get_cache[s // 4]:
                copy.wait()
        rows = slice(s * 16, (s + 1) * 16)
        q_s = heads_q[rows, :]
        scores = jnp.dot(q_s, keys[s], preferred_element_type=jnp.float32) * score_scale
        length = len_ref[s]
        sums = logsum[s]
        last = jnp.sum(jnp.where(position == length - 1, sums, 0.0), axis=-1, keepdims=True)
        forget = jnp.sum(
            jnp.where(diagonal, jnp.broadcast_to(gate_col[s : s + 1, :], (16, 16)), 0.0), axis=-1, keepdims=True
        )
        new_sum = last + forget
        logsum_out[s : s + 1, :] = jnp.sum(
            jnp.where(diagonal, jnp.broadcast_to(new_sum, (16, 16)), 0.0), axis=0, keepdims=True
        )
        scores = jnp.where(position < length, scores + new_sum - sums, -jnp.inf)
        own_score = (
            jnp.sum(q_s.astype(jnp.float32) * own_col[s : s + 1, :], axis=-1, keepdims=True) * score_scale
        )
        top = jnp.maximum(jnp.max(scores, axis=-1, keepdims=True), own_score)
        past = jnp.exp(scores - top)
        own_exp = jnp.exp(own_score - top)
        share = 1.0 / (jnp.sum(past, axis=-1, keepdims=True) + own_exp)
        past_weight = (past * share).astype(jnp.bfloat16)
        own_weight = (own_exp * share).astype(jnp.bfloat16).astype(jnp.float32)
        attended = lax.dot_general(
            past_weight, values[s], (((1,), (1,)), ((), ())), preferred_element_type=jnp.float32
        )
        att_rows[rows, :] = (attended + own_weight * new_val[s : s + 1, :]).astype(jnp.bfloat16)
        if s % 8 == 7:
            piece = s // 8
            wide = lax.dot_general(
                att_rows[piece * 128 : (piece + 1) * 128, :],
                fold,
                (((1,), (1,)), ((), ())),
                preferred_element_type=jnp.float32,
            )
            for i in range(8):
                att_flat[i : i + 1, :] = jnp.sum(
                    jnp.where(own_lanes, wide[i * 16 : (i + 1) * 16, :], 0.0), axis=0, keepdims=True
                )
            att_ref[piece * 8 : (piece + 1) * 8, :] = att_flat[...].astype(jnp.bfloat16)
            over_z(lambda d, zz, piece=piece: send_att(piece, d, zz).start())
    aall[0, pair] = att_ref[...]

    with jax.named_scope("d_info"):
        over_z(lambda d, zz: z_copy(3, info_ref.at[0], infoall.at[zz], zz, d, zz).wait_recv())
    info = jnp.sum(infoall[...], axis=0)
    row = lax.broadcasted_iota(jnp.int32, (256, 128), 0)
    token = lax.broadcasted_iota(jnp.int32, (256, 128), 1)
    expert = (lax.rem(row, 128) // 8 + z * PLANE).astype(jnp.float32)
    named = jnp.zeros((256, 128), jnp.float32)
    scale = jnp.zeros((256, 128), jnp.float32)
    for j in range(TOP_K):
        hit = info[j : j + 1, :] == expert
        named = named + jnp.where(hit, 1.0, 0.0)
        scale = scale + jnp.where(hit, info[8 + j : 9 + j, :], 0.0)
    first = lax.broadcasted_iota(jnp.int32, (128, 128), 0)
    second = lax.broadcasted_iota(jnp.int32, (128, 128), 1)
    ahead = jnp.where((first // ROWS == second // ROWS) & (first < second), 1.0, 0.0).astype(jnp.bfloat16)
    rank = jnp.dot(named.astype(jnp.bfloat16), ahead, preferred_element_type=jnp.float32)
    slot = lax.rem(row, 2).astype(jnp.float32)
    here = (row // 128) * 4 + lax.rem(row, 8) // 2 == token // ROWS
    pick = jnp.where(here & (rank == slot), named, 0.0)
    combine = jnp.transpose(pick * scale)
    picks = [pick[0:128, 0:64].astype(jnp.bfloat16), pick[128:256, 64:128].astype(jnp.bfloat16)]
    combine_high, combine_low = [], []
    for j in range(2):
        part_of = combine[j * 64 : (j + 1) * 64, j * 128 : (j + 1) * 128]
        combine_high.append(part_of.astype(jnp.bfloat16))
        combine_low.append((part_of - combine_high[j].astype(jnp.float32)).astype(jnp.bfloat16))

    get_wo.wait()
    with jax.named_scope("b_w"):
        over_plane(lambda d, pp: p_copy(0, wo_ref.at[:, my_columns], wall.at[pp], pp, d, pp).wait_recv())
    with jax.named_scope("c_att"):
        for piece in range(2):
            rows = pl.ds(piece * 8, 8)
            over_z(
                lambda d, zz, piece=piece, rows=rows: z_copy(
                    piece, att_ref.at[rows], aall.at[lax.rem(d, 2), zz // 2, rows], zz, d, zz
                ).wait_recv()
            )

    att = aall[...].reshape(NZ * ROWS, HALF)
    for h in range(2):
        weights = wall[h * 8 : (h + 1) * 8].reshape(128, HALF)
        part[h] = lax.dot_general(att, weights, (((1,), (1,)), ((), ())), preferred_element_type=jnp.float32)
    give = t_copy(0, part.at[o], part_in)
    give.start()
    with jax.named_scope("e_hid"):
        over_z(lambda d, zz: z_copy(2, hid_block(zz), hcol.at[lax.rem(d, 2), zz // 2], zz, d, zz).wait_recv())
    with jax.named_scope("e_give"):
        give.wait_recv()
    mixed_now = (part[t] + part_in[...]).astype(jnp.bfloat16)
    mixed[...] = mixed_now.reshape(2, 4, ROWS, 128)
    residual = hcol[...].reshape(NZ * ROWS, 128).astype(jnp.float32) + mixed_now.astype(jnp.float32)
    rounded[...] = residual.astype(jnp.bfloat16).reshape(2, 4, ROWS, 128)

    def send_rounded(j, d, zz):
        return z_copy(4 + j, rounded.at[lax.rem(d + j, 2)], rall.at[j, z], zz, d, z)

    def send_mixed(d, zz):
        return z_copy(6, mixed.at[lax.rem(d, 2), zz // 2], mown.at[z], zz, d, z)

    for j in range(2):
        over_z(lambda d, zz, j=j: send_rounded(j, d, zz).start())
        rall[j, z] = rounded[j]
    over_z(lambda d, zz: send_mixed(d, zz).start())
    mown[z] = mixed[0, pair]

    def send_rows(j, d, pp):
        return p_copy(1 + j, disp.at[j, pp], xrow.at[t, j, me], pp, d, me)

    def forward(j, pp):
        return pltpu.make_async_remote_copy(
            src_ref=xrow.at[t, j, pp],
            dst_ref=xrow.at[t, j, pp],
            send_sem=f_send.at[j, pp],
            recv_sem=f_recv.at[j, pp],
            device_id={"tp": o},
            device_id_type=MESH,
        )

    def arrival(j, pp):
        return pltpu.make_async_remote_copy(
            src_ref=xrow.at[o, j, pp],
            dst_ref=xrow.at[o, j, pp],
            send_sem=f_send.at[j, pp],
            recv_sem=f_recv.at[j, pp],
            device_id={"tp": o},
            device_id_type=MESH,
        )

    give_sq = [t_copy(1 + j, sq.at[j], sq_in.at[j]) for j in range(2)]
    for j in range(2):
        with jax.named_scope(f"g_mixed#j={j}"):
            over_z(lambda d, zz, j=j: z_copy(4 + j, rounded.at[0], rall.at[j, zz], zz, d, zz).wait_recv())
        squares = jnp.zeros((64, 128), jnp.float32)
        for zz in range(NZ):
            block = rall[j, zz].reshape(64, 128).astype(jnp.float32)
            squares = squares + block * block
        sq[j] = jnp.broadcast_to(jnp.sum(squares, axis=-1, keepdims=True), (64, 128))
        give_sq[j].start()
        with jax.named_scope(f"h_sq#j={j}"):
            give_sq[j].wait_recv()
        inverse = lax.rsqrt((sq[j] + sq_in[j]) * (1.0 / WIDE) + epsilon)
        for zz in range(NZ):
            gain = gains[1, pl.ds(2 * zz + t, 1), :]
            block = rall[j, zz].reshape(64, 128).astype(jnp.float32)
            block = (block * inverse * gain).astype(jnp.bfloat16)
            rows = jnp.dot(picks[j], block, preferred_element_type=jnp.float32)
            disp[j, :, :, zz * 128 : (zz + 1) * 128] = rows.astype(jnp.bfloat16).reshape(PLANE, 8, 128)
        over_plane(lambda d, pp, j=j: send_rows(j, d, pp).start())
        xrow[t, j, me] = disp[j, me]
        forward(j, me).start()

    def send_ret(j, d, pp):
        return p_copy(3 + j, ret.at[j, pp], back.at[j, me], pp, d, me)

    give_o = [t_copy(3 + j, o_out.at[j], o_in.at[j]) for j in range(2)]
    for j in range(2):

        def pass_on(d, pp, j=j):
            p_copy(1 + j, disp.at[j, pp], xrow.at[t, j, pp], pp, d, pp).wait_recv()
            forward(j, pp).start()

        with jax.named_scope(f"i_disp#j={j}"):
            over_plane(pass_on)
        if j == 0:
            for load in loads:
                load.wait()
        mine = xrow[t, j].reshape(128, HALF)
        gate_act = jnp.dot(mine, gate_v[t], preferred_element_type=jnp.float32)
        up_act = jnp.dot(mine, up_v[t], preferred_element_type=jnp.float32)
        with jax.named_scope(f"k_fwd#j={j}"):
            lax.fori_loop(0, PLANE, lambda i, c, j=j: (arrival(j, i).wait_recv(), c)[1], 0)
        other = xrow[o, j].reshape(128, HALF)
        gate_act = gate_act + jnp.dot(other, gate_v[o], preferred_element_type=jnp.float32)
        up_act = up_act + jnp.dot(other, up_v[o], preferred_element_type=jnp.float32)
        act = (gate_act * (1.0 / (1.0 + jnp.exp(-gate_act))) * up_act).astype(jnp.bfloat16)
        o_out[j] = jnp.dot(act, down_v[o], preferred_element_type=jnp.float32).astype(jnp.bfloat16)
        give_o[j].start()
        own = jnp.dot(act, down_v[t], preferred_element_type=jnp.float32).astype(jnp.bfloat16)
        with jax.named_scope(f"l_o#j={j}"):
            give_o[j].wait_recv()
        both = own.astype(jnp.float32) + o_in[j].astype(jnp.float32)
        ret[j] = both.astype(jnp.bfloat16).reshape(PLANE, 8, HALF)
        over_plane(lambda d, pp, j=j: send_ret(j, d, pp).start())
        back[j, me] = ret[j, me]

    def send_sum(j, d, zz):
        return z_copy(7, psum.at[j, zz // 2], tsum.at[z], zz, d, z)

    for j in range(2):
        with jax.named_scope(f"m_ret#j={j}"):
            over_plane(lambda d, pp, j=j: p_copy(3 + j, ret.at[j, pp], back.at[j, pp], pp, d, pp).wait_recv())
        outs = back[j].reshape(128, HALF)
        total = jnp.dot(combine_high[j], outs, preferred_element_type=jnp.float32)
        total = total + jnp.dot(combine_low[j], outs, preferred_element_type=jnp.float32)
        psum[j] = total.astype(jnp.bfloat16).reshape(4, ROWS, HALF)
        for d in range(1, NZ):
            if d % 2 == j:
                send_sum(j, d, lax.rem(z + d, NZ)).start()
        if j == 0:
            tsum[z] = psum[0, pair]
    over_z(lambda d, zz: z_copy(6, mixed.at[0, 0], mown.at[zz], zz, d, zz).wait_recv())
    with jax.named_scope("n_z"):
        over_z(lambda d, zz: z_copy(7, psum.at[0, 0], tsum.at[zz], zz, d, zz).wait_recv())
    mix = jnp.sum(tsum[...].astype(jnp.float32), axis=0)
    for zz in range(NZ):
        block = hid_block(zz)[...].astype(jnp.float32) + mown[zz].astype(jnp.float32)
        upd[:, zz * 128 : (zz + 1) * 128] = (block + mix[:, zz * 128 : (zz + 1) * 128]).astype(jnp.bfloat16)
    give_u = t_copy(5, upd, upd_in)
    give_u.start()
    for zz in range(NZ):
        out_ref[:, pl.ds(pl.multiple_of(zz * 256 + t * 128, 128), 128)] = upd[:, zz * 128 : (zz + 1) * 128]
    with jax.named_scope("o_u"):
        give_u.wait_recv()
    for zz in range(NZ):
        out_ref[:, pl.ds(pl.multiple_of(zz * 256 + o * 128, 128), 128)] = upd_in[:, zz * 128 : (zz + 1) * 128]

    with jax.named_scope("p_sends"):
        over_plane(lambda d, pp: send_wo(d, pp).wait_send())
        over_z(lambda d, zz: send_hid(d, zz).wait_send())
        over_z(lambda d, zz: send_info(d, zz).wait_send())
        over_z(lambda d, zz: send_mixed(d, zz).wait_send())
        for j in range(2):
            over_z(lambda d, zz, j=j: send_att(j, d, zz).wait_send())
            over_z(lambda d, zz, j=j: send_rounded(j, d, zz).wait_send())
            over_plane(lambda d, pp, j=j: send_rows(j, d, pp).wait_send())
            over_plane(lambda d, pp, j=j: send_ret(j, d, pp).wait_send())
            lax.fori_loop(0, PLANE, lambda i, c, j=j: (forward(j, i).wait_send(), c)[1], 0)
        over_z(lambda d, zz: send_sum(0, d, zz).wait_send())
        for give_one in [give, give_u] + give_sq + give_o:
            give_one.wait_send()


def layer(lengths, *arrays):
    bf16, f32 = jnp.bfloat16, jnp.float32
    vmem = pl.BlockSpec(memory_space=pltpu.VMEM)
    hbm = pl.BlockSpec(memory_space=pl.ANY)
    dma = pltpu.SemaphoreType.DMA
    return pl.pallas_call(
        layer_kernel,
        out_shape=(
            jax.ShapeDtypeStruct((ROWS, WIDE), bf16),
            jax.ShapeDtypeStruct((ROWS, HD), bf16),
            jax.ShapeDtypeStruct((ROWS, HD), bf16),
            jax.ShapeDtypeStruct((ROWS, 16), f32),
        ),
        in_specs=[pl.BlockSpec(memory_space=pltpu.SMEM)] + [vmem] * 5 + [hbm] * 12,
        out_specs=(vmem,) * 4,
        scratch_shapes=[
            pltpu.VMEM((ROWS, WIDE), bf16),
            pltpu.VMEM((WIDE, HALF), bf16),
            pltpu.VMEM((144, WIDE), bf16),
            pltpu.VMEM((ROWS, HD, 1024), bf16),
            pltpu.VMEM((ROWS, HD, 1024), bf16),
            pltpu.VMEM((ROWS, 16, 1024), f32),
            pltpu.VMEM((ROWS, WIDE), bf16),
            pltpu.VMEM((ROWS, HALF), f32),
            pltpu.VMEM((256, HALF), bf16),
            pltpu.VMEM((256, HD), bf16),
            pltpu.VMEM((ROWS, 16), f32),
            pltpu.VMEM((ROWS, HD), f32),
            pltpu.VMEM((ROWS, HD), f32),
            pltpu.VMEM((256, HD), bf16),
            pltpu.VMEM((8, HALF), f32),
            pltpu.VMEM((ROWS, HALF), bf16),
            pltpu.VMEM((2, 16, 128), f32),
            pltpu.VMEM((2, 16, 128), f32),
            pltpu.VMEM((NZ, 16, 128), f32),
            pltpu.VMEM((PLANE, ROWS, HALF), bf16),
            pltpu.VMEM((2, 4, ROWS, HALF), bf16),
            pltpu.VMEM((2, 4, ROWS, 128), bf16),
            pltpu.VMEM((2, NZ * ROWS, 128), f32),
            pltpu.VMEM((NZ * ROWS, 128), f32),
            pltpu.VMEM((2, 4, ROWS, 128), bf16),
            pltpu.VMEM((2, 4, ROWS, 128), bf16),
            pltpu.VMEM((NZ, ROWS, 128), bf16),
            pltpu.VMEM((2, NZ, 4, ROWS, 128), bf16),
            pltpu.VMEM((2, 64, 128), f32),
            pltpu.VMEM((2, 64, 128), f32),
            pltpu.VMEM((2, PLANE, 8, HALF), bf16),
            pltpu.VMEM((2, 2, PLANE, 8, HALF), bf16),
            pltpu.VMEM((2, HALF, 256), bf16),
            pltpu.VMEM((2, HALF, 256), bf16),
            pltpu.VMEM((2, 256, HALF), bf16),
            pltpu.VMEM((2, 128, HALF), bf16),
            pltpu.VMEM((2, 128, HALF), bf16),
            pltpu.VMEM((2, PLANE, 8, HALF), bf16),
            pltpu.VMEM((2, PLANE, 8, HALF), bf16),
            pltpu.VMEM((2, 4, ROWS, HALF), bf16),
            pltpu.VMEM((NZ, ROWS, HALF), bf16),
            pltpu.VMEM((ROWS, HALF), bf16),
            pltpu.VMEM((ROWS, HALF), bf16),
            dma((8, NZ)),
            dma((8, NZ)),
            dma((5, PLANE)),
            dma((5, PLANE)),
            dma((2, PLANE)),
            dma((2, PLANE)),
            dma((6,)),
            dma((6,)),
            dma((3, 16)),
            dma((21,)),
        ],
        compiler_params=pltpu.CompilerParams(
            collective_id=0, has_side_effects=True, vmem_limit_bytes=56 * 1024 * 1024
        ),
    )(lengths, *arrays)


def hand_over(*refs):
    for source, target in zip(refs[:4], refs[4:]):
        target[...] = source[...]


def write_out(*results):
    vmem = pl.BlockSpec(memory_space=pltpu.VMEM)
    return pl.pallas_call(
        hand_over,
        out_shape=tuple(jax.ShapeDtypeStruct(r.shape, r.dtype) for r in results),
        in_specs=[vmem] * 4,
        out_specs=(vmem,) * 4,
    )(*results)


def per_device(
    hidden,
    attn_gain,
    query_weight,
    key_weight,
    value_weight,
    forget_weight,
    forget_bias,
    cache_keys,
    cache_values,
    cache_logsum,
    lengths,
    out_weight,
    ffn_gain,
    expert_ids,
    expert_scores,
    gate_weights,
    up_weights,
    down_weights,
):
    results = layer(
        lengths,
        attn_gain,
        ffn_gain,
        forget_bias,
        expert_ids.T,
        expert_scores.T,
        hidden,
        query_weight,
        key_weight.T,
        value_weight.T,
        forget_weight.T,
        cache_keys,
        cache_values,
        cache_logsum,
        out_weight,
        gate_weights,
        up_weights,
        down_weights,
    )
    updated, key_new, value_new, new_logsum = write_out(*results)
    return (updated, key_new[:, None, :], value_new[:, None, :], new_logsum)


def solution(mesh):
    split = Mesh(mesh.devices.reshape(8, 4, 4, mesh.shape["tp"]), ("ep_0", "ep_1", "ep_2", "tp"))
    in_specs = (
        P(EP, None),
        P(),
        P(None, "tp"),
        P(None, "tp"),
        P(None, "tp"),
        P(None, "tp"),
        P("tp"),
        P(EP, "tp", None, None),
        P(EP, "tp", None, None),
        P(EP, "tp", None),
        P(EP),
        P(EP, None),
        P(),
        P(EP, None),
        P(EP, None),
        P(EP, None, "tp"),
        P(EP, None, "tp"),
        P(EP, "tp", None),
    )
    out_specs = (P(EP, None), P(EP, "tp", None), P(EP, "tp", None), P(EP, "tp"))
    return jax.shard_map(
        per_device, mesh=split, in_specs=in_specs, out_specs=out_specs, check_vma=False
    )
```

time: 83.8 us -> 65.3 us (0.78)
  Pallas kernels: 70.2 us -> 64.5 us
  matrix products: 5.67 us -> 0 us
  other arithmetic: 3.74 us -> 0 us
  local copies, waits for them, and re-layouts: 3.03 us -> 0 us
    pallas_call x1 -> x2, Pallas kernels: 70.2 us -> 64.5 us  [the longest x1 63 us: layer(): pl.pallas_call(layer_kernel, out_shape=(jax.ShapeDtypeStruct((ROWS, WIDE)...]
    dot_general x7 -> x0, matrix products: 5.67 us -> none  [the longest x1 3.01 us: per_device(): jnp.dot(normed, query_weight, preferred_element_type=jnp.float32)]
    unnamed x29 -> x0, local copies, waits for them, and re-layouts: 1.95 us -> none
    reduce_sum x4 -> x0, other arithmetic: 1.49 us -> none  [the longest x1 0.97 us: root_norm(): jnp.mean(floats * floats, axis=-1, keepdims=True) + epsilon]
    convert_element_type x2 -> x0, other arithmetic: 0.85 us -> none  [the longest x1 0.84 us: root_norm(): return floats * inv_root * gain.astype(jnp.float32)]
where the time goes in v2:
time: 65.3 us; the launch traced here: 65.2 us
  Pallas kernels  64.5 us (99%)
    pallas_call x1, Pallas kernels, layer(): pl.pallas_call(layer_kernel, out_shape=(jax.ShapeDtypeStruct((ROWS, WIDE)...  63 us
    pallas_call x1, Pallas kernels, write_out(): pl.pallas_call(hand_over, out_shape=tuple((jax.ShapeDtypeStruct(r.shape,...  1.49 us

profile of v2, /device:TPU:1, one launch (start us, length us, event | category | flops | bytes accessed | tf_op | source)
XLA Modules:
  0.0 65.2 jit_solution(10739643355469813107)
XLA Ops:
  0.6 63.0 %shard_map.201 = (bf16[16,2048]{1,0:T(8,128)(2,1)}, bf16[16,64]{1,0:T(8,128)(2,1)}, bf16[16,64]{1,0:T(8,128)(2,1)}, f32[16,16]{1,0:T(8,128)}) custom-call(s32[16]{0:T(128)} %len_ref.1, bf16[2048]{0:T(1024)(128)(2,1)} %attn_gain_ref.1, bf16[2048]{0:T(1024)(128)(2,1)} %ffn_gain_ref.1, f32[16]{0:T(128)} %bias_ref.1, s32[6,16]{1,0:T(8,128)} %bitcast.10, ...), custom_call_target="tpu_custom_call" | custom-call | tf_op jit(solution)/shard_map/pallas_call | solution.py:540
  63.7 1.5 %shard_map.202 = (bf16[16,2048]{1,0:T(8,128)(2,1)}, bf16[16,64]{1,0:T(8,128)(2,1)}, bf16[16,64]{1,0:T(8,128)(2,1)}, f32[16,16]{1,0:T(8,128)}) custom-call(bf16[16,2048]{1,0:T(8,128)(2,1)} %get-tuple-element.12.refs_0_, bf16[16,64]{1,0:T(8,128)(2,1)} %get-tuple-element.13.refs_1_, bf16[16,64]{1,0:T(8,128)(2,1)} %get-tuple-element.14.refs_2_, ...), custom_call_target="tpu_custom_call" | custom-call | tf_op jit(solution)/shard_map/pallas_call | solution.py:618

commit v3 on v2

--- a/solution.py
+++ b/solution.py
@@ -71,8 +71,8 @@
     rounded,
     mown,
     rall,
-    sq,
-    sq_in,
+    ss,
+    ssall,
     disp,
     xrow,
     gate_v,
@@ -106,22 +106,22 @@
     parity = lax.rem(z, 2)
     pair = z // 2
 
-    def z_copy(phase, src, dst, zz, i, slot):
+    def z_copy(phase, src, dst, zz):
         return pltpu.make_async_remote_copy(
             src_ref=src,
             dst_ref=dst,
-            send_sem=z_send.at[phase, i],
-            recv_sem=z_recv.at[phase, slot],
+            send_sem=z_send.at[phase],
+            recv_sem=z_recv.at[phase],
             device_id={"ep_0": zz},
             device_id_type=MESH,
         )
 
-    def p_copy(phase, src, dst, pp, i, slot):
+    def p_copy(phase, src, dst, pp, arrive):
         return pltpu.make_async_remote_copy(
             src_ref=src,
             dst_ref=dst,
-            send_sem=p_send.at[phase, i],
-            recv_sem=p_recv.at[phase, slot],
+            send_sem=p_send.at[phase],
+            recv_sem=p_recv.at[arrive],
             device_id={"ep_1": pp // NX, "ep_2": lax.rem(pp, NX)},
             device_id_type=MESH,
         )
@@ -136,19 +136,29 @@
             device_id_type=MESH,
         )
 
+    z_steps = (4, 3, 5, 2, 6, 1, 7)
+    p_steps = sorted(
+        ((dy, dx) for dy in range(4) for dx in range(4) if dy or dx),
+        key=lambda d: -(min(d[0], 4 - d[0]) + min(d[1], 4 - d[1])),
+    )
+
     def over_z(fn):
-        def step(d, carry):
+        for d in z_steps:
             fn(d, lax.rem(z + d, NZ))
-            return carry
-
-        lax.fori_loop(1, NZ, step, 0)
 
     def over_plane(fn):
-        def step(d, carry):
-            fn(d, lax.rem(me + d, PLANE))
-            return carry
-
-        lax.fori_loop(1, PLANE, step, 0)
+        for i, (dy, dx) in enumerate(p_steps):
+            fn(i, lax.rem(y + dy, 4) * NX + lax.rem(x + dx, 4))
+
+    def source(i):
+        dy, dx = p_steps[i]
+        return lax.rem(y + 4 - dy, 4) * NX + lax.rem(x + 4 - dx, 4)
+
+    def z_wait(phase, ref):
+        z_copy(phase, ref, ref, lax.rem(z + 1, NZ)).wait_recv()
+
+    def p_wait(arrive, ref):
+        p_copy(0, ref, ref, lax.rem(me + 1, PLANE), arrive).wait_recv()
 
     get_hid = pltpu.make_async_copy(hid_hbm, hid_ref, a_sem.at[0])
     get_hid.start()
@@ -214,7 +224,10 @@
     def hid_block(zz):
         return hid_ref.at[:, pl.ds(pl.multiple_of(zz * 256 + t * 128, 128), 128)]
 
-    hcol[0, pair] = hid_block(z)[...]
+    def hid_cols(zz):
+        return hid_ref.at[:, pl.ds(pl.multiple_of(zz * 256, 256), 256)]
+
+    hcol[pair] = hid_cols(z)[...]
 
     query = jnp.zeros((ROWS, HALF), jnp.float32)
     for i in range(4):
@@ -226,34 +239,35 @@
         )
     queries[...] = query.astype(jnp.bfloat16).astype(jnp.float32)
 
-    with jax.named_scope("a_barrier"):
-        pl.semaphore_wait(barrier, (NZ - 1) + (PLANE - 1) + 1)
     get_wo = pltpu.make_async_copy(wo_ref.at[:, my_columns], wall.at[me], a_sem.at[20])
     get_wo.start()
-
-    def send_wo(d, pp):
-        return p_copy(0, wo_ref.at[:, my_columns], wall.at[me], pp, d, me)
-
-    def send_hid(d, zz):
-        return z_copy(2, hid_block(zz), hcol.at[lax.rem(d, 2), pair], zz, d, z)
-
-    def send_info(d, zz):
-        return z_copy(3, info_ref.at[lax.rem(zz, 2)], infoall.at[z], zz, d, z)
-
-    over_plane(lambda d, pp: send_wo(d, pp).start())
-    over_z(lambda d, zz: send_hid(d, zz).start())
-    over_z(lambda d, zz: send_info(d, zz).start())
     loads = []
     for zz in range(NZ):
         for h in range(2):
             rows = pl.ds(zz * 256 + h * 128, 128)
             put = pl.ds(zz * 128, 128)
             n = zz * 2 + h
-            loads.append(pltpu.make_async_copy(gate_ref.at[0, rows, :], gate_v.at[h, put, :], w_sem.at[0, n]))
-            loads.append(pltpu.make_async_copy(up_ref.at[0, rows, :], up_v.at[h, put, :], w_sem.at[1, n]))
-            loads.append(pltpu.make_async_copy(down_ref.at[0, :, rows], down_v.at[h, :, put], w_sem.at[2, n]))
-    for load in loads:
-        load.start()
+            loads.append(pltpu.make_async_copy(gate_ref.at[0, rows, :], gate_v.at[h, put, :], w_sem.at[0]))
+            loads.append(pltpu.make_async_copy(up_ref.at[0, rows, :], up_v.at[h, put, :], w_sem.at[1]))
+            loads.append(pltpu.make_async_copy(down_ref.at[0, :, rows], down_v.at[h, :, put], w_sem.at[2]))
+
+    def send_wo(i, pp):
+        return p_copy(0, wo_ref.at[:, my_columns], wall.at[me], pp, 0)
+
+    def send_hid(d, zz):
+        return z_copy(2, hid_cols(zz), hcol.at[(d % 2) * 4 + pair], zz)
+
+    def send_info(d, zz):
+        return z_copy(3, info_ref.at[lax.rem(zz, 2)], infoall.at[z], zz)
+
+    def greet():
+        with jax.named_scope("a_barrier"):
+            pl.semaphore_wait(barrier, (NZ - 1) + (PLANE - 1) + 1)
+        over_plane(lambda i, pp: send_wo(i, pp).start())
+        over_z(lambda d, zz: send_hid(d, zz).start())
+        over_z(lambda d, zz: send_info(d, zz).start())
+        for load in loads:
+            load.start()
 
     for copy in get_small:
         copy.wait()
@@ -290,9 +304,11 @@
 
     def send_att(piece, d, zz):
         rows = pl.ds(piece * 8, 8)
-        return z_copy(piece, att_ref.at[rows], aall.at[lax.rem(d, 2), pair, rows], zz, d, z)
+        return z_copy(piece, att_ref.at[rows], aall.at[(d % 2) * 4 + pair, rows], zz)
 
     for s in range(ROWS):
+        if s == 4:
+            greet()
         if s % 4 == 0:
             for copy in get_cache[s // 4]:
                 copy.wait()
@@ -337,10 +353,10 @@
                 )
             att_ref[piece * 8 : (piece + 1) * 8, :] = att_flat[...].astype(jnp.bfloat16)
             over_z(lambda d, zz, piece=piece: send_att(piece, d, zz).start())
-    aall[0, pair] = att_ref[...]
+    aall[pair] = att_ref[...]
 
     with jax.named_scope("d_info"):
-        over_z(lambda d, zz: z_copy(3, info_ref.at[0], infoall.at[zz], zz, d, zz).wait_recv())
+        z_wait(3, infoall.at[pl.ds(0, 7)])
     info = jnp.sum(infoall[...], axis=0)
     row = lax.broadcasted_iota(jnp.int32, (256, 128), 0)
     token = lax.broadcasted_iota(jnp.int32, (256, 128), 1)
@@ -368,146 +384,166 @@
 
     get_wo.wait()
     with jax.named_scope("b_w"):
-        over_plane(lambda d, pp: p_copy(0, wo_ref.at[:, my_columns], wall.at[pp], pp, d, pp).wait_recv())
+        p_wait(0, wall.at[pl.ds(0, 15)])
     with jax.named_scope("c_att"):
         for piece in range(2):
-            rows = pl.ds(piece * 8, 8)
-            over_z(
-                lambda d, zz, piece=piece, rows=rows: z_copy(
-                    piece, att_ref.at[rows], aall.at[lax.rem(d, 2), zz // 2, rows], zz, d, zz
-                ).wait_recv()
-            )
+            z_wait(piece, aall.at[pl.ds(0, 7), pl.ds(piece * 8, 8)])
 
     att = aall[...].reshape(NZ * ROWS, HALF)
     for h in range(2):
         weights = wall[h * 8 : (h + 1) * 8].reshape(128, HALF)
         part[h] = lax.dot_general(att, weights, (((1,), (1,)), ((), ())), preferred_element_type=jnp.float32)
-    give = t_copy(0, part.at[o], part_in)
+    give = t_copy(0, part, part_in)
     give.start()
     with jax.named_scope("e_hid"):
-        over_z(lambda d, zz: z_copy(2, hid_block(zz), hcol.at[lax.rem(d, 2), zz // 2], zz, d, zz).wait_recv())
+        z_wait(2, hcol.at[pl.ds(0, 7)])
     with jax.named_scope("e_give"):
         give.wait_recv()
-    mixed_now = (part[t] + part_in[...]).astype(jnp.bfloat16)
-    mixed[...] = mixed_now.reshape(2, 4, ROWS, 128)
-    residual = hcol[...].reshape(NZ * ROWS, 128).astype(jnp.float32) + mixed_now.astype(jnp.float32)
-    rounded[...] = residual.astype(jnp.bfloat16).reshape(2, 4, ROWS, 128)
+    squares = jnp.zeros((NZ * ROWS, 128), jnp.float32)
+    for h in range(2):
+        mixed_now = (part[h] + part_in[h]).astype(jnp.bfloat16)
+        hid_now = hcol[:, :, h * 128 : (h + 1) * 128].reshape(NZ * ROWS, 128).astype(jnp.float32)
+        residual = hid_now + mixed_now.astype(jnp.float32)
+        squares = squares + residual * residual
+        mixed[h] = mixed_now.reshape(8, ROWS, 128)
+        rounded[h] = residual.astype(jnp.bfloat16).reshape(2, 4, ROWS, 128)
 
     def send_rounded(j, d, zz):
-        return z_copy(4 + j, rounded.at[lax.rem(d + j, 2)], rall.at[j, z], zz, d, z)
+        return z_copy(4 + j, rounded.at[t, (d + j) % 2], rall.at[j, z], zz)
 
     def send_mixed(d, zz):
-        return z_copy(6, mixed.at[lax.rem(d, 2), zz // 2], mown.at[z], zz, d, z)
-
+        return z_copy(6, mixed.at[t, (d % 2) * 4 + zz // 2], mown.at[z], zz)
+
+    def send_ss(d, zz):
+        return z_copy(8, ss.at[d % 2], ssall.at[z], zz)
+
+    over_z(lambda d, zz: send_rounded(0, d, zz).start())
+    sums = lax.dot_general(
+        jnp.ones((8, 128), jnp.float32),
+        squares,
+        (((1,), (1,)), ((), ())),
+        precision=lax.Precision.HIGHEST,
+        preferred_element_type=jnp.float32,
+    )
+    ss[0] = sums
+    ss[1] = pltpu.roll(sums, 64, 1)
+    over_z(lambda d, zz: send_ss(d, zz).start())
+    over_z(lambda d, zz: send_rounded(1, d, zz).start())
+    over_z(lambda d, zz: send_mixed(d, zz).start())
+    ssall[z] = ss[0]
     for j in range(2):
-        over_z(lambda d, zz, j=j: send_rounded(j, d, zz).start())
-        rall[j, z] = rounded[j]
-    over_z(lambda d, zz: send_mixed(d, zz).start())
-    mown[z] = mixed[0, pair]
-
-    def send_rows(j, d, pp):
-        return p_copy(1 + j, disp.at[j, pp], xrow.at[t, j, me], pp, d, me)
+        rall[j, z] = rounded[t, j]
+    mown[z] = mixed[t, pair]
+
+    def send_rows(j, i, pp):
+        return p_copy(1 + j, disp.at[j, pp], xrow.at[t, j, me], pp, 5 + j * 3 + i // 5)
 
     def forward(j, pp):
         return pltpu.make_async_remote_copy(
             src_ref=xrow.at[t, j, pp],
             dst_ref=xrow.at[t, j, pp],
-            send_sem=f_send.at[j, pp],
-            recv_sem=f_recv.at[j, pp],
+            send_sem=f_send.at[j],
+            recv_sem=f_recv.at[j],
             device_id={"tp": o},
             device_id_type=MESH,
         )
 
-    def arrival(j, pp):
+    def forwarded(j, ref):
         return pltpu.make_async_remote_copy(
-            src_ref=xrow.at[o, j, pp],
-            dst_ref=xrow.at[o, j, pp],
-            send_sem=f_send.at[j, pp],
-            recv_sem=f_recv.at[j, pp],
+            src_ref=ref,
+            dst_ref=ref,
+            send_sem=f_send.at[j],
+            recv_sem=f_recv.at[j],
             device_id={"tp": o},
             device_id_type=MESH,
         )
 
-    give_sq = [t_copy(1 + j, sq.at[j], sq_in.at[j]) for j in range(2)]
     for j in range(2):
         with jax.named_scope(f"g_mixed#j={j}"):
-            over_z(lambda d, zz, j=j: z_copy(4 + j, rounded.at[0], rall.at[j, zz], zz, d, zz).wait_recv())
-        squares = jnp.zeros((64, 128), jnp.float32)
-        for zz in range(NZ):
-            block = rall[j, zz].reshape(64, 128).astype(jnp.float32)
-            squares = squares + block * block
-        sq[j] = jnp.broadcast_to(jnp.sum(squares, axis=-1, keepdims=True), (64, 128))
-        give_sq[j].start()
-        with jax.named_scope(f"h_sq#j={j}"):
-            give_sq[j].wait_recv()
-        inverse = lax.rsqrt((sq[j] + sq_in[j]) * (1.0 / WIDE) + epsilon)
+            if j == 0:
+                z_wait(8, ssall.at[pl.ds(0, 7)])
+            z_wait(4 + j, rall.at[j, pl.ds(0, 7)])
+        if j == 0:
+            inverse = lax.rsqrt(jnp.sum(ssall[...], axis=0)[0:1, :] * (1.0 / WIDE) + epsilon)
+            factor = jnp.sum(pick * inverse, axis=-1, keepdims=True)
         for zz in range(NZ):
             gain = gains[1, pl.ds(2 * zz + t, 1), :]
-            block = rall[j, zz].reshape(64, 128).astype(jnp.float32)
-            block = (block * inverse * gain).astype(jnp.bfloat16)
-            rows = jnp.dot(picks[j], block, preferred_element_type=jnp.float32)
+            rows = jnp.dot(picks[j], rall[j, zz].reshape(64, 128), preferred_element_type=jnp.float32)
+            rows = rows * factor[j * 128 : (j + 1) * 128] * gain
             disp[j, :, :, zz * 128 : (zz + 1) * 128] = rows.astype(jnp.bfloat16).reshape(PLANE, 8, 128)
-        over_plane(lambda d, pp, j=j: send_rows(j, d, pp).start())
+        over_plane(lambda i, pp, j=j: send_rows(j, i, pp).start())
         xrow[t, j, me] = disp[j, me]
         forward(j, me).start()
 
-    def send_ret(j, d, pp):
-        return p_copy(3 + j, ret.at[j, pp], back.at[j, me], pp, d, me)
-
-    give_o = [t_copy(3 + j, o_out.at[j], o_in.at[j]) for j in range(2)]
-    for j in range(2):
-
-        def pass_on(d, pp, j=j):
-            p_copy(1 + j, disp.at[j, pp], xrow.at[t, j, pp], pp, d, pp).wait_recv()
-            forward(j, pp).start()
-
+    def send_ret(j, i, pp):
+        return p_copy(3 + j, ret.at[j, pp], back.at[j, me], pp, 3 + j)
+
+    def take(j):
         with jax.named_scope(f"i_disp#j={j}"):
-            over_plane(pass_on)
-        if j == 0:
-            for load in loads:
-                load.wait()
+            for g in range(3):
+                p_wait(5 + j * 3 + g, xrow.at[t, j, pl.ds(0, 5)])
+                for i in range(g * 5, g * 5 + 5):
+                    forward(j, source(i)).start()
+
+    def first_half(j):
         mine = xrow[t, j].reshape(128, HALF)
         gate_act = jnp.dot(mine, gate_v[t], preferred_element_type=jnp.float32)
-        up_act = jnp.dot(mine, up_v[t], preferred_element_type=jnp.float32)
+        return gate_act, jnp.dot(mine, up_v[t], preferred_element_type=jnp.float32)
+
+    give_o = [t_copy(1 + j, o_out.at[j], o_in.at[j]) for j in range(2)]
+
+    def second_half(j, gate_act, up_act):
         with jax.named_scope(f"k_fwd#j={j}"):
-            lax.fori_loop(0, PLANE, lambda i, c, j=j: (arrival(j, i).wait_recv(), c)[1], 0)
+            forwarded(j, xrow.at[o, j]).wait_recv()
         other = xrow[o, j].reshape(128, HALF)
         gate_act = gate_act + jnp.dot(other, gate_v[o], preferred_element_type=jnp.float32)
         up_act = up_act + jnp.dot(other, up_v[o], preferred_element_type=jnp.float32)
         act = (gate_act * (1.0 / (1.0 + jnp.exp(-gate_act))) * up_act).astype(jnp.bfloat16)
         o_out[j] = jnp.dot(act, down_v[o], preferred_element_type=jnp.float32).astype(jnp.bfloat16)
         give_o[j].start()
-        own = jnp.dot(act, down_v[t], preferred_element_type=jnp.float32).astype(jnp.bfloat16)
+        return jnp.dot(act, down_v[t], preferred_element_type=jnp.float32).astype(jnp.bfloat16)
+
+    def give_back(j, own):
         with jax.named_scope(f"l_o#j={j}"):
             give_o[j].wait_recv()
         both = own.astype(jnp.float32) + o_in[j].astype(jnp.float32)
         ret[j] = both.astype(jnp.bfloat16).reshape(PLANE, 8, HALF)
-        over_plane(lambda d, pp, j=j: send_ret(j, d, pp).start())
+        over_plane(lambda i, pp: send_ret(j, i, pp).start())
         back[j, me] = ret[j, me]
 
+    for n, whole in enumerate((gate_v, up_v, down_v)):
+        pltpu.make_async_copy(whole, whole, w_sem.at[n]).wait()
+    take(0)
+    own_0 = second_half(0, *first_half(0))
+    take(1)
+    acts = first_half(1)
+    give_back(0, own_0)
+    own_1 = second_half(1, *acts)
+    give_back(1, own_1)
+
     def send_sum(j, d, zz):
-        return z_copy(7, psum.at[j, zz // 2], tsum.at[z], zz, d, z)
+        return z_copy(7, psum.at[j, zz // 2], tsum.at[z], zz)
 
     for j in range(2):
         with jax.named_scope(f"m_ret#j={j}"):
-            over_plane(lambda d, pp, j=j: p_copy(3 + j, ret.at[j, pp], back.at[j, pp], pp, d, pp).wait_recv())
+            p_wait(3 + j, back.at[j, pl.ds(0, 15)])
         outs = back[j].reshape(128, HALF)
         total = jnp.dot(combine_high[j], outs, preferred_element_type=jnp.float32)
         total = total + jnp.dot(combine_low[j], outs, preferred_element_type=jnp.float32)
         psum[j] = total.astype(jnp.bfloat16).reshape(4, ROWS, HALF)
-        for d in range(1, NZ):
+        for d in z_steps:
             if d % 2 == j:
                 send_sum(j, d, lax.rem(z + d, NZ)).start()
         if j == 0:
             tsum[z] = psum[0, pair]
-    over_z(lambda d, zz: z_copy(6, mixed.at[0, 0], mown.at[zz], zz, d, zz).wait_recv())
+    z_wait(6, mown.at[pl.ds(0, 7)])
     with jax.named_scope("n_z"):
-        over_z(lambda d, zz: z_copy(7, psum.at[0, 0], tsum.at[zz], zz, d, zz).wait_recv())
+        z_wait(7, tsum.at[pl.ds(0, 7)])
     mix = jnp.sum(tsum[...].astype(jnp.float32), axis=0)
     for zz in range(NZ):
         block = hid_block(zz)[...].astype(jnp.float32) + mown[zz].astype(jnp.float32)
         upd[:, zz * 128 : (zz + 1) * 128] = (block + mix[:, zz * 128 : (zz + 1) * 128]).astype(jnp.bfloat16)
-    give_u = t_copy(5, upd, upd_in)
+    give_u = t_copy(3, upd, upd_in)
     give_u.start()
     for zz in range(NZ):
         out_ref[:, pl.ds(pl.multiple_of(zz * 256 + t * 128, 128), 128)] = upd[:, zz * 128 : (zz + 1) * 128]
@@ -517,33 +553,47 @@
         out_ref[:, pl.ds(pl.multiple_of(zz * 256 + o * 128, 128), 128)] = upd_in[:, zz * 128 : (zz + 1) * 128]
 
     with jax.named_scope("p_sends"):
-        over_plane(lambda d, pp: send_wo(d, pp).wait_send())
-        over_z(lambda d, zz: send_hid(d, zz).wait_send())
-        over_z(lambda d, zz: send_info(d, zz).wait_send())
-        over_z(lambda d, zz: send_mixed(d, zz).wait_send())
+        next_z, next_p = lax.rem(z + 1, NZ), lax.rem(me + 1, PLANE)
+        sent = (
+            aall.at[pl.ds(0, 7), pl.ds(0, 8)],
+            aall.at[pl.ds(0, 7), pl.ds(8, 8)],
+            hcol.at[pl.ds(0, 7)],
+            infoall.at[pl.ds(0, 7)],
+            rall.at[0, pl.ds(0, 7)],
+            rall.at[1, pl.ds(0, 7)],
+            mown.at[pl.ds(0, 7)],
+            tsum.at[pl.ds(0, 7)],
+            ssall.at[pl.ds(0, 7)],
+        )
+        for phase, ref in enumerate(sent):
+            z_copy(phase, ref, ref, next_z).wait_send()
+        sent = (
+            wall.at[pl.ds(0, 15)],
+            disp.at[0, pl.ds(0, 15)],
+            disp.at[1, pl.ds(0, 15)],
+            ret.at[0, pl.ds(0, 15)],
+            ret.at[1, pl.ds(0, 15)],
+        )
+        for phase, ref in enumerate(sent):
+            p_copy(phase, ref, ref, next_p, 0).wait_send()
         for j in range(2):
-            over_z(lambda d, zz, j=j: send_att(j, d, zz).wait_send())
-            over_z(lambda d, zz, j=j: send_rounded(j, d, zz).wait_send())
-            over_plane(lambda d, pp, j=j: send_rows(j, d, pp).wait_send())
-            over_plane(lambda d, pp, j=j: send_ret(j, d, pp).wait_send())
-            lax.fori_loop(0, PLANE, lambda i, c, j=j: (forward(j, i).wait_send(), c)[1], 0)
-        over_z(lambda d, zz: send_sum(0, d, zz).wait_send())
-        for give_one in [give, give_u] + give_sq + give_o:
+            forwarded(j, xrow.at[t, j]).wait_send()
+        for give_one in [give, give_u] + give_o:
             give_one.wait_send()
 
 
 def layer(lengths, *arrays):
     bf16, f32 = jnp.bfloat16, jnp.float32
     vmem = pl.BlockSpec(memory_space=pltpu.VMEM)
-    hbm = pl.BlockSpec(memory_space=pl.ANY)
+    hbm = pl.BlockSpec(memory_space=pltpu.HBM)
     dma = pltpu.SemaphoreType.DMA
     return pl.pallas_call(
         layer_kernel,
         out_shape=(
-            jax.ShapeDtypeStruct((ROWS, WIDE), bf16),
-            jax.ShapeDtypeStruct((ROWS, HD), bf16),
-            jax.ShapeDtypeStruct((ROWS, HD), bf16),
-            jax.ShapeDtypeStruct((ROWS, 16), f32),
+            pltpu.VMEM((ROWS, WIDE), bf16),
+            pltpu.VMEM((ROWS, HD), bf16),
+            pltpu.VMEM((ROWS, HD), bf16),
+            pltpu.VMEM((ROWS, 16), f32),
         ),
         in_specs=[pl.BlockSpec(memory_space=pltpu.SMEM)] + [vmem] * 5 + [hbm] * 12,
         out_specs=(vmem,) * 4,
@@ -568,16 +618,16 @@
             pltpu.VMEM((2, 16, 128), f32),
             pltpu.VMEM((NZ, 16, 128), f32),
             pltpu.VMEM((PLANE, ROWS, HALF), bf16),
-            pltpu.VMEM((2, 4, ROWS, HALF), bf16),
-            pltpu.VMEM((2, 4, ROWS, 128), bf16),
+            pltpu.VMEM((8, ROWS, HALF), bf16),
+            pltpu.VMEM((8, ROWS, 256), bf16),
             pltpu.VMEM((2, NZ * ROWS, 128), f32),
-            pltpu.VMEM((NZ * ROWS, 128), f32),
-            pltpu.VMEM((2, 4, ROWS, 128), bf16),
-            pltpu.VMEM((2, 4, ROWS, 128), bf16),
+            pltpu.VMEM((2, NZ * ROWS, 128), f32),
+            pltpu.VMEM((2, 8, ROWS, 128), bf16),
+            pltpu.VMEM((2, 2, 4, ROWS, 128), bf16),
             pltpu.VMEM((NZ, ROWS, 128), bf16),
             pltpu.VMEM((2, NZ, 4, ROWS, 128), bf16),
-            pltpu.VMEM((2, 64, 128), f32),
-            pltpu.VMEM((2, 64, 128), f32),
+            pltpu.VMEM((2, 8, 128), f32),
+            pltpu.VMEM((NZ, 8, 128), f32),
             pltpu.VMEM((2, PLANE, 8, HALF), bf16),
             pltpu.VMEM((2, 2, PLANE, 8, HALF), bf16),
             pltpu.VMEM((2, HALF, 256), bf16),
@@ -591,15 +641,15 @@
             pltpu.VMEM((NZ, ROWS, HALF), bf16),
             pltpu.VMEM((ROWS, HALF), bf16),
             pltpu.VMEM((ROWS, HALF), bf16),
-            dma((8, NZ)),
-            dma((8, NZ)),
-            dma((5, PLANE)),
-            dma((5, PLANE)),
-            dma((2, PLANE)),
-            dma((2, PLANE)),
-            dma((6,)),
-            dma((6,)),
-            dma((3, 16)),
+            dma((9,)),
+            dma((9,)),
+            dma((5,)),
+            dma((11,)),
+            dma((2,)),
+            dma((2,)),
+            dma((4,)),
+            dma((4,)),
+            dma((3,)),
             dma((21,)),
         ],
         compiler_params=pltpu.CompilerParams(
@@ -620,6 +670,7 @@
         out_shape=tuple(jax.ShapeDtypeStruct(r.shape, r.dtype) for r in results),
         in_specs=[vmem] * 4,
         out_specs=(vmem,) * 4,
+        compiler_params=pltpu.CompilerParams(vmem_limit_bytes=1024 * 1024),
     )(*results)
 
 

time: 65.3 us -> 58 us (0.89)
  Pallas kernels: 64.5 us -> 57.2 us
    pallas_call x1, Pallas kernels: 63 us -> 56.6 us  [layer(): pl.pallas_call(layer_kernel, out_shape=(pltpu.VMEM((ROWS, WIDE), bf16), p...]
    pallas_call x1, Pallas kernels: 1.49 us -> 0.65 us  [write_out(): pl.pallas_call(hand_over, out_shape=tuple((jax.ShapeDtypeStruct(r.shape,...]
where the time goes in v3:
time: 58 us; the launch traced here: 57.9 us
  Pallas kernels  57.2 us (99%)
  between operations  0.65 us (1%)
    pallas_call x1, Pallas kernels, layer(): pl.pallas_call(layer_kernel, out_shape=(pltpu.VMEM((ROWS, WIDE), bf16), p...  56.6 us

profile of v3, /device:TPU:1, one launch (start us, length us, event | category | flops | bytes accessed | tf_op | source)
XLA Modules:
  0.0 57.9 jit_solution(15974342679977031009)
XLA Ops:
  0.6 56.6 %shard_map.201 = (bf16[16,2048]{1,0:T(8,128)(2,1)S(1)}, bf16[16,64]{1,0:T(8,128)(2,1)S(1)}, bf16[16,64]{1,0:T(8,128)(2,1)S(1)}, f32[16,16]{1,0:T(8,128)S(1)}) custom-call(s32[16]{0:T(128)} %len_ref.1, bf16[2048]{0:T(1024)(128)(2,1)} %attn_gain_ref.1, bf16[2048]{0:T(1024)(128)(2,1)} %ffn_gain_ref.1, f32[16]{0:T(128)} %bias_ref.1, s32[6,16]{1,0:T(8,128)} %bitcast.10, ...), custom_call_target="tpu_custom_call" | custom-call | tf_op jit(solution)/shard_map/pallas_call | solution.py:590
  57.2 0.6 %shard_map.202 = (bf16[16,2048]{1,0:T(8,128)(2,1)}, bf16[16,64]{1,0:T(8,128)(2,1)}, bf16[16,64]{1,0:T(8,128)(2,1)}, f32[16,16]{1,0:T(8,128)}) custom-call(bf16[16,2048]{1,0:T(8,128)(2,1)S(1)} %get-tuple-element.12.refs_0_, bf16[16,64]{1,0:T(8,128)(2,1)S(1)} %get-tuple-element.13.refs_1_, bf16[16,64]{1,0:T(8,128)(2,1)S(1)} %get-tuple-element.14.refs_2_, ...), custom_call_target="tpu_custom_call" | custom-call | tf_op jit(solution)/shard_map/pallas_call | solution.py:668

commit v4 on v3

--- a/solution.py
+++ b/solution.py
@@ -78,8 +78,9 @@
     gate_v,
     up_v,
     down_v,
-    o_out,
-    o_in,
+    gate_p,
+    up_p,
+    down_p,
     ret,
     back,
     psum,
@@ -90,8 +91,6 @@
     z_recv,
     p_send,
     p_recv,
-    f_send,
-    f_recv,
     t_send,
     t_recv,
     w_sem,
@@ -116,13 +115,13 @@
             device_id_type=MESH,
         )
 
-    def p_copy(phase, src, dst, pp, arrive):
+    def p_copy(phase, src, dst, pp, arrive, core):
         return pltpu.make_async_remote_copy(
             src_ref=src,
             dst_ref=dst,
             send_sem=p_send.at[phase],
             recv_sem=p_recv.at[arrive],
-            device_id={"ep_1": pp // NX, "ep_2": lax.rem(pp, NX)},
+            device_id={"ep_1": pp // NX, "ep_2": lax.rem(pp, NX), "tp": core},
             device_id_type=MESH,
         )
 
@@ -150,15 +149,11 @@
         for i, (dy, dx) in enumerate(p_steps):
             fn(i, lax.rem(y + dy, 4) * NX + lax.rem(x + dx, 4))
 
-    def source(i):
-        dy, dx = p_steps[i]
-        return lax.rem(y + 4 - dy, 4) * NX + lax.rem(x + 4 - dx, 4)
-
     def z_wait(phase, ref):
         z_copy(phase, ref, ref, lax.rem(z + 1, NZ)).wait_recv()
 
     def p_wait(arrive, ref):
-        p_copy(0, ref, ref, lax.rem(me + 1, PLANE), arrive).wait_recv()
+        p_copy(0, ref, ref, lax.rem(me + 1, PLANE), arrive, t).wait_recv()
 
     get_hid = pltpu.make_async_copy(hid_hbm, hid_ref, a_sem.at[0])
     get_hid.start()
@@ -189,24 +184,22 @@
 
     barrier = pltpu.get_barrier_semaphore()
     over_z(lambda d, zz: pl.semaphore_signal(barrier, inc=1, device_id={"ep_0": zz}, device_id_type=MESH))
-    over_plane(
-        lambda d, pp: pl.semaphore_signal(
-            barrier,
-            inc=1,
-            device_id={"ep_1": pp // NX, "ep_2": lax.rem(pp, NX)},
-            device_id_type=MESH,
-        )
-    )
+    for core in range(2):
+        over_plane(
+            lambda d, pp, core=core: pl.semaphore_signal(
+                barrier,
+                inc=1,
+                device_id={"ep_1": pp // NX, "ep_2": lax.rem(pp, NX), "tp": core},
+                device_id_type=MESH,
+            )
+        )
     pl.semaphore_signal(barrier, inc=1, device_id={"tp": o}, device_id_type=MESH)
 
-    info_ref[...] = jnp.zeros((2, 16, 128), jnp.float32)
+    info_ref[...] = jnp.zeros((8, 128), jnp.float32)
+    info_ref[0:TOP_K, 0:ROWS] = ids_ref[...].astype(jnp.float32)
     shares = scores_ref[...] / jnp.sum(scores_ref[...], axis=0, keepdims=True)
-    info_ref[0, 0:TOP_K, 0:ROWS] = ids_ref[...].astype(jnp.float32)
-    info_ref[0, 8 : 8 + TOP_K, 0:ROWS] = shares
-    facts = info_ref[0]
-    info_ref[0] = pltpu.roll(facts, pair * ROWS + parity * 64, 1)
-    info_ref[1] = pltpu.roll(facts, pair * ROWS + (1 - parity) * 64, 1)
-    infoall[z] = info_ref[parity]
+    info_ref[0:TOP_K, ROWS : 2 * ROWS] = shares
+    infoall[z] = info_ref[...]
     gains[0] = attn_gain_ref[...].astype(jnp.float32).reshape(16, 128)
     gains[1] = ffn_gain_ref[...].astype(jnp.float32).reshape(16, 128)
 
@@ -252,20 +245,19 @@
             loads.append(pltpu.make_async_copy(down_ref.at[0, :, rows], down_v.at[h, :, put], w_sem.at[2]))
 
     def send_wo(i, pp):
-        return p_copy(0, wo_ref.at[:, my_columns], wall.at[me], pp, 0)
+        return p_copy(0, wo_ref.at[:, my_columns], wall.at[me], pp, 0, t)
 
     def send_hid(d, zz):
         return z_copy(2, hid_cols(zz), hcol.at[(d % 2) * 4 + pair], zz)
 
     def send_info(d, zz):
-        return z_copy(3, info_ref.at[lax.rem(zz, 2)], infoall.at[z], zz)
+        return z_copy(3, info_ref, infoall.at[z], zz)
 
     def greet():
         with jax.named_scope("a_barrier"):
-            pl.semaphore_wait(barrier, (NZ - 1) + (PLANE - 1) + 1)
+            pl.semaphore_wait(barrier, (NZ - 1) + 2 * (PLANE - 1) + 1)
         over_plane(lambda i, pp: send_wo(i, pp).start())
         over_z(lambda d, zz: send_hid(d, zz).start())
-        over_z(lambda d, zz: send_info(d, zz).start())
         for load in loads:
             load.start()
 
@@ -353,34 +345,14 @@
                 )
             att_ref[piece * 8 : (piece + 1) * 8, :] = att_flat[...].astype(jnp.bfloat16)
             over_z(lambda d, zz, piece=piece: send_att(piece, d, zz).start())
+    over_z(lambda d, zz: send_info(d, zz).start())
     aall[pair] = att_ref[...]
-
-    with jax.named_scope("d_info"):
-        z_wait(3, infoall.at[pl.ds(0, 7)])
-    info = jnp.sum(infoall[...], axis=0)
-    row = lax.broadcasted_iota(jnp.int32, (256, 128), 0)
-    token = lax.broadcasted_iota(jnp.int32, (256, 128), 1)
-    expert = (lax.rem(row, 128) // 8 + z * PLANE).astype(jnp.float32)
-    named = jnp.zeros((256, 128), jnp.float32)
-    scale = jnp.zeros((256, 128), jnp.float32)
-    for j in range(TOP_K):
-        hit = info[j : j + 1, :] == expert
-        named = named + jnp.where(hit, 1.0, 0.0)
-        scale = scale + jnp.where(hit, info[8 + j : 9 + j, :], 0.0)
-    first = lax.broadcasted_iota(jnp.int32, (128, 128), 0)
-    second = lax.broadcasted_iota(jnp.int32, (128, 128), 1)
-    ahead = jnp.where((first // ROWS == second // ROWS) & (first < second), 1.0, 0.0).astype(jnp.bfloat16)
-    rank = jnp.dot(named.astype(jnp.bfloat16), ahead, preferred_element_type=jnp.float32)
-    slot = lax.rem(row, 2).astype(jnp.float32)
-    here = (row // 128) * 4 + lax.rem(row, 8) // 2 == token // ROWS
-    pick = jnp.where(here & (rank == slot), named, 0.0)
-    combine = jnp.transpose(pick * scale)
-    picks = [pick[0:128, 0:64].astype(jnp.bfloat16), pick[128:256, 64:128].astype(jnp.bfloat16)]
-    combine_high, combine_low = [], []
-    for j in range(2):
-        part_of = combine[j * 64 : (j + 1) * 64, j * 128 : (j + 1) * 128]
-        combine_high.append(part_of.astype(jnp.bfloat16))
-        combine_low.append((part_of - combine_high[j].astype(jnp.float32)).astype(jnp.bfloat16))
+    wholes = ((gate_v, gate_p), (up_v, up_p), (down_v, down_p))
+    swaps = []
+    for n, (mine, theirs) in enumerate(wholes):
+        pltpu.make_async_copy(mine, mine, w_sem.at[n]).wait()
+        swaps.append(t_copy(2 + n, mine, theirs))
+        swaps[n].start()
 
     get_wo.wait()
     with jax.named_scope("b_w"):
@@ -435,28 +407,43 @@
         rall[j, z] = rounded[t, j]
     mown[z] = mixed[t, pair]
 
+    with jax.named_scope("d_info"):
+        z_wait(3, infoall.at[pl.ds(0, 7)])
+    lane = lax.broadcasted_iota(jnp.int32, (8, 128), 1)
+    routes = jnp.zeros((8, 128), jnp.float32)
+    weights_of = jnp.zeros((8, 128), jnp.float32)
+    for zz in range(NZ):
+        tile = infoall[zz]
+        place = (lax.rem(z + zz, 2) * 4 + zz // 2) * ROWS
+        routes = routes + pltpu.roll(jnp.where(lane < ROWS, tile, 0.0), place, 1)
+        tile = jnp.where((lane >= ROWS) & (lane < 2 * ROWS), tile, 0.0)
+        weights_of = weights_of + pltpu.roll(tile, lax.rem(place + 128 - ROWS, 128), 1)
+    row = lax.broadcasted_iota(jnp.int32, (256, 128), 0)
+    token = lax.broadcasted_iota(jnp.int32, (256, 128), 1)
+    expert = (lax.rem(row, 128) // 8 + z * PLANE).astype(jnp.float32)
+    named = jnp.zeros((256, 128), jnp.float32)
+    scale = jnp.zeros((256, 128), jnp.float32)
+    for j in range(TOP_K):
+        hit = routes[j : j + 1, :] == expert
+        named = named + jnp.where(hit, 1.0, 0.0)
+        scale = scale + jnp.where(hit, weights_of[j : j + 1, :], 0.0)
+    first = lax.broadcasted_iota(jnp.int32, (128, 128), 0)
+    second = lax.broadcasted_iota(jnp.int32, (128, 128), 1)
+    ahead = jnp.where((first // ROWS == second // ROWS) & (first < second), 1.0, 0.0).astype(jnp.bfloat16)
+    rank = jnp.dot(named.astype(jnp.bfloat16), ahead, preferred_element_type=jnp.float32)
+    slot = lax.rem(row, 2).astype(jnp.float32)
+    here = (row // 128) * 4 + lax.rem(row, 8) // 2 == token // ROWS
+    pick = jnp.where(here & (rank == slot), named, 0.0)
+    combine = jnp.transpose(pick * scale)
+    picks = [pick[0:128, 0:64].astype(jnp.bfloat16), pick[128:256, 64:128].astype(jnp.bfloat16)]
+    combine_high, combine_low = [], []
+    for j in range(2):
+        part_of = combine[j * 64 : (j + 1) * 64, j * 128 : (j + 1) * 128]
+        combine_high.append(part_of.astype(jnp.bfloat16))
+        combine_low.append((part_of - combine_high[j].astype(jnp.float32)).astype(jnp.bfloat16))
+
     def send_rows(j, i, pp):
-        return p_copy(1 + j, disp.at[j, pp], xrow.at[t, j, me], pp, 5 + j * 3 + i // 5)
-
-    def forward(j, pp):
-        return pltpu.make_async_remote_copy(
-            src_ref=xrow.at[t, j, pp],
-            dst_ref=xrow.at[t, j, pp],
-            send_sem=f_send.at[j],
-            recv_sem=f_recv.at[j],
-            device_id={"tp": o},
-            device_id_type=MESH,
-        )
-
-    def forwarded(j, ref):
-        return pltpu.make_async_remote_copy(
-            src_ref=ref,
-            dst_ref=ref,
-            send_sem=f_send.at[j],
-            recv_sem=f_recv.at[j],
-            device_id={"tp": o},
-            device_id_type=MESH,
-        )
+        return p_copy(1 + j, disp.at[j, pp], xrow.at[t, me], pp, 1 + t, j)
 
     for j in range(2):
         with jax.named_scope(f"g_mixed#j={j}"):
@@ -472,78 +459,84 @@
             rows = rows * factor[j * 128 : (j + 1) * 128] * gain
             disp[j, :, :, zz * 128 : (zz + 1) * 128] = rows.astype(jnp.bfloat16).reshape(PLANE, 8, 128)
         over_plane(lambda i, pp, j=j: send_rows(j, i, pp).start())
-        xrow[t, j, me] = disp[j, me]
-        forward(j, me).start()
-
-    def send_ret(j, i, pp):
-        return p_copy(3 + j, ret.at[j, pp], back.at[j, me], pp, 3 + j)
-
-    def take(j):
-        with jax.named_scope(f"i_disp#j={j}"):
-            for g in range(3):
-                p_wait(5 + j * 3 + g, xrow.at[t, j, pl.ds(0, 5)])
-                for i in range(g * 5, g * 5 + 5):
-                    forward(j, source(i)).start()
-
-    def first_half(j):
-        mine = xrow[t, j].reshape(128, HALF)
-        gate_act = jnp.dot(mine, gate_v[t], preferred_element_type=jnp.float32)
-        return gate_act, jnp.dot(mine, up_v[t], preferred_element_type=jnp.float32)
-
-    give_o = [t_copy(1 + j, o_out.at[j], o_in.at[j]) for j in range(2)]
-
-    def second_half(j, gate_act, up_act):
-        with jax.named_scope(f"k_fwd#j={j}"):
-            forwarded(j, xrow.at[o, j]).wait_recv()
-        other = xrow[o, j].reshape(128, HALF)
-        gate_act = gate_act + jnp.dot(other, gate_v[o], preferred_element_type=jnp.float32)
-        up_act = up_act + jnp.dot(other, up_v[o], preferred_element_type=jnp.float32)
-        act = (gate_act * (1.0 / (1.0 + jnp.exp(-gate_act))) * up_act).astype(jnp.bfloat16)
-        o_out[j] = jnp.dot(act, down_v[o], preferred_element_type=jnp.float32).astype(jnp.bfloat16)
-        give_o[j].start()
-        return jnp.dot(act, down_v[t], preferred_element_type=jnp.float32).astype(jnp.bfloat16)
-
-    def give_back(j, own):
-        with jax.named_scope(f"l_o#j={j}"):
-            give_o[j].wait_recv()
-        both = own.astype(jnp.float32) + o_in[j].astype(jnp.float32)
-        ret[j] = both.astype(jnp.bfloat16).reshape(PLANE, 8, HALF)
-        over_plane(lambda i, pp: send_ret(j, i, pp).start())
-        back[j, me] = ret[j, me]
-
-    for n, whole in enumerate((gate_v, up_v, down_v)):
-        pltpu.make_async_copy(whole, whole, w_sem.at[n]).wait()
-    take(0)
-    own_0 = second_half(0, *first_half(0))
-    take(1)
-    acts = first_half(1)
-    give_back(0, own_0)
-    own_1 = second_half(1, *acts)
-    give_back(1, own_1)
-
-    def send_sum(j, d, zz):
-        return z_copy(7, psum.at[j, zz // 2], tsum.at[z], zz)
-
+
+    xrow[t, me] = disp[t, me]
+
+    def to_other(phase, src, dst, arrive):
+        return pltpu.make_async_remote_copy(
+            src_ref=src,
+            dst_ref=dst,
+            send_sem=t_send.at[phase],
+            recv_sem=p_recv.at[arrive],
+            device_id={"tp": o},
+            device_id_type=MESH,
+        )
+
+    give_rows = to_other(5, disp.at[o, me], xrow.at[t, me], 1 + t)
+    give_rows.start()
+    for swap in swaps:
+        swap.wait_recv()
+    with jax.named_scope("i_disp"):
+        p_wait(1 + t, xrow.at[t, pl.ds(0, 15)])
+        p_wait(1 + o, xrow.at[o])
+
+    rows_in = [xrow[h].reshape(128, HALF) for h in range(2)]
+
+    def hidden_act(gate_w, up_w):
+        gate_act = jnp.dot(rows_in[0], gate_w[0], preferred_element_type=jnp.float32)
+        gate_act = gate_act + jnp.dot(rows_in[1], gate_w[1], preferred_element_type=jnp.float32)
+        up_act = jnp.dot(rows_in[0], up_w[0], preferred_element_type=jnp.float32)
+        up_act = up_act + jnp.dot(rows_in[1], up_w[1], preferred_element_type=jnp.float32)
+        return (gate_act * (1.0 / (1.0 + jnp.exp(-gate_act))) * up_act).astype(jnp.bfloat16)
+
+    act_mine = hidden_act(gate_v, up_v)
+    act_theirs = hidden_act(gate_p, up_p)
+
+    def send_ret(h, q, i, pp):
+        return p_copy(3 + h * 2 + q, ret.at[h, q, pp], back.at[t, q, me], pp, 3 + t * 2 + q, h)
+
+    def give_ret(q):
+        return t_copy(6 + q, ret.at[o, q, me], back.at[t, q, me])
+
+    for q in range(2):
+        for h in range(2):
+            columns = slice(q * 512, (q + 1) * 512)
+            one = jnp.dot(act_mine, down_v[h, :, columns], preferred_element_type=jnp.float32)
+            two = jnp.dot(act_theirs, down_p[h, :, columns], preferred_element_type=jnp.float32)
+            both = one.astype(jnp.bfloat16).astype(jnp.float32) + two.astype(jnp.bfloat16).astype(jnp.float32)
+            ret[h, q] = both.astype(jnp.bfloat16).reshape(PLANE, 8, 512)
+            over_plane(lambda i, pp, h=h, q=q: send_ret(h, q, i, pp).start())
+        give_ret(q).start()
+        back[t, q, me] = ret[t, q, me]
+
+    def send_sum(j, q, d, zz):
+        return z_copy(7 + 2 * q, psum.at[j, q, zz // 2], tsum.at[q, z], zz)
+
+    for q in range(2):
+        give_ret(q).wait_recv()
     for j in range(2):
-        with jax.named_scope(f"m_ret#j={j}"):
-            p_wait(3 + j, back.at[j, pl.ds(0, 15)])
-        outs = back[j].reshape(128, HALF)
-        total = jnp.dot(combine_high[j], outs, preferred_element_type=jnp.float32)
-        total = total + jnp.dot(combine_low[j], outs, preferred_element_type=jnp.float32)
-        psum[j] = total.astype(jnp.bfloat16).reshape(4, ROWS, HALF)
-        for d in z_steps:
-            if d % 2 == j:
-                send_sum(j, d, lax.rem(z + d, NZ)).start()
-        if j == 0:
-            tsum[z] = psum[0, pair]
+        for q in range(2):
+            with jax.named_scope(f"m_ret#j={j}#q={q}"):
+                p_wait(3 + j * 2 + q, back.at[j, q, pl.ds(0, 15)])
+            outs = back[j, q].reshape(128, 512)
+            total = jnp.dot(combine_high[j], outs, preferred_element_type=jnp.float32)
+            total = total + jnp.dot(combine_low[j], outs, preferred_element_type=jnp.float32)
+            psum[j, q] = total.astype(jnp.bfloat16).reshape(4, ROWS, 512)
+            for d in z_steps:
+                if d % 2 == j:
+                    send_sum(j, q, d, lax.rem(z + d, NZ)).start()
+            if j == 0:
+                tsum[q, z] = psum[0, q, pair]
     z_wait(6, mown.at[pl.ds(0, 7)])
-    with jax.named_scope("n_z"):
-        z_wait(7, tsum.at[pl.ds(0, 7)])
-    mix = jnp.sum(tsum[...].astype(jnp.float32), axis=0)
-    for zz in range(NZ):
-        block = hid_block(zz)[...].astype(jnp.float32) + mown[zz].astype(jnp.float32)
-        upd[:, zz * 128 : (zz + 1) * 128] = (block + mix[:, zz * 128 : (zz + 1) * 128]).astype(jnp.bfloat16)
-    give_u = t_copy(3, upd, upd_in)
+    for q in range(2):
+        with jax.named_scope(f"n_z#q={q}"):
+            z_wait(7 + 2 * q, tsum.at[q, pl.ds(0, 7)])
+        mix = jnp.sum(tsum[q].astype(jnp.float32), axis=0)
+        for i in range(4):
+            zz = q * 4 + i
+            block = hid_block(zz)[...].astype(jnp.float32) + mown[zz].astype(jnp.float32)
+            upd[:, zz * 128 : (zz + 1) * 128] = (block + mix[:, i * 128 : (i + 1) * 128]).astype(jnp.bfloat16)
+    give_u = t_copy(1, upd, upd_in)
     give_u.start()
     for zz in range(NZ):
         out_ref[:, pl.ds(pl.multiple_of(zz * 256 + t * 128, 128), 128)] = upd[:, zz * 128 : (zz + 1) * 128]
@@ -562,23 +555,17 @@
             rall.at[0, pl.ds(0, 7)],
             rall.at[1, pl.ds(0, 7)],
             mown.at[pl.ds(0, 7)],
-            tsum.at[pl.ds(0, 7)],
+            tsum.at[0, pl.ds(0, 7)],
             ssall.at[pl.ds(0, 7)],
+            tsum.at[1, pl.ds(0, 7)],
         )
         for phase, ref in enumerate(sent):
             z_copy(phase, ref, ref, next_z).wait_send()
-        sent = (
-            wall.at[pl.ds(0, 15)],
-            disp.at[0, pl.ds(0, 15)],
-            disp.at[1, pl.ds(0, 15)],
-            ret.at[0, pl.ds(0, 15)],
-            ret.at[1, pl.ds(0, 15)],
-        )
+        sent = [wall.at[pl.ds(0, 15)], disp.at[0, pl.ds(0, 15)], disp.at[1, pl.ds(0, 15)]]
+        sent += [ret.at[h, q, pl.ds(0, 15)] for h in range(2) for q in range(2)]
         for phase, ref in enumerate(sent):
-            p_copy(phase, ref, ref, next_p, 0).wait_send()
-        for j in range(2):
-            forwarded(j, xrow.at[t, j]).wait_send()
-        for give_one in [give, give_u] + give_o:
+            p_copy(phase, ref, ref, next_p, 0, t).wait_send()
+        for give_one in [give, give_u, give_rows, give_ret(0), give_ret(1)] + swaps:
             give_one.wait_send()
 
 
@@ -615,8 +602,8 @@
             pltpu.VMEM((8, HALF), f32),
             pltpu.VMEM((ROWS, HALF), bf16),
             pltpu.VMEM((2, 16, 128), f32),
-            pltpu.VMEM((2, 16, 128), f32),
-            pltpu.VMEM((NZ, 16, 128), f32),
+            pltpu.VMEM((8, 128), f32),
+            pltpu.VMEM((NZ, 8, 128), f32),
             pltpu.VMEM((PLANE, ROWS, HALF), bf16),
             pltpu.VMEM((8, ROWS, HALF), bf16),
             pltpu.VMEM((8, ROWS, 256), bf16),
@@ -629,26 +616,25 @@
             pltpu.VMEM((2, 8, 128), f32),
             pltpu.VMEM((NZ, 8, 128), f32),
             pltpu.VMEM((2, PLANE, 8, HALF), bf16),
-            pltpu.VMEM((2, 2, PLANE, 8, HALF), bf16),
+            pltpu.VMEM((2, PLANE, 8, HALF), bf16),
             pltpu.VMEM((2, HALF, 256), bf16),
             pltpu.VMEM((2, HALF, 256), bf16),
             pltpu.VMEM((2, 256, HALF), bf16),
-            pltpu.VMEM((2, 128, HALF), bf16),
-            pltpu.VMEM((2, 128, HALF), bf16),
-            pltpu.VMEM((2, PLANE, 8, HALF), bf16),
-            pltpu.VMEM((2, PLANE, 8, HALF), bf16),
-            pltpu.VMEM((2, 4, ROWS, HALF), bf16),
-            pltpu.VMEM((NZ, ROWS, HALF), bf16),
+            pltpu.VMEM((2, HALF, 256), bf16),
+            pltpu.VMEM((2, HALF, 256), bf16),
+            pltpu.VMEM((2, 256, HALF), bf16),
+            pltpu.VMEM((2, 2, PLANE, 8, 512), bf16),
+            pltpu.VMEM((2, 2, PLANE, 8, 512), bf16),
+            pltpu.VMEM((2, 2, 4, ROWS, 512), bf16),
+            pltpu.VMEM((2, NZ, ROWS, 512), bf16),
             pltpu.VMEM((ROWS, HALF), bf16),
             pltpu.VMEM((ROWS, HALF), bf16),
-            dma((9,)),
-            dma((9,)),
-            dma((5,)),
-            dma((11,)),
-            dma((2,)),
-            dma((2,)),
-            dma((4,)),
-            dma((4,)),
+            dma((10,)),
+            dma((10,)),
+            dma((7,)),
+            dma((7,)),
+            dma((8,)),
+            dma((8,)),
             dma((3,)),
             dma((21,)),
         ],

time: 58 us -> 56.9 us (0.981)
  Pallas kernels: 57.2 us -> 56.1 us
    pallas_call x1, Pallas kernels: 56.6 us -> 55.5 us  [layer(): pl.pallas_call(layer_kernel, out_shape=(pltpu.VMEM((ROWS, WIDE), bf16), p...]
where the time goes in v4:
time: 56.9 us; the launch traced here: 56.8 us
  Pallas kernels  56.1 us (99%)
  between operations  0.65 us (1%)
    pallas_call x1, Pallas kernels, layer(): pl.pallas_call(layer_kernel, out_shape=(pltpu.VMEM((ROWS, WIDE), bf16), p...  55.5 us

profile of v4, /device:TPU:1, one launch (start us, length us, event | category | flops | bytes accessed | tf_op | source)
XLA Modules:
  0.0 56.8 jit_solution(8948186139170269208)
XLA Ops:
  0.6 55.5 %shard_map.201 = (bf16[16,2048]{1,0:T(8,128)(2,1)S(1)}, bf16[16,64]{1,0:T(8,128)(2,1)S(1)}, bf16[16,64]{1,0:T(8,128)(2,1)S(1)}, f32[16,16]{1,0:T(8,128)S(1)}) custom-call(s32[16]{0:T(128)} %len_ref.1, bf16[2048]{0:T(1024)(128)(2,1)} %attn_gain_ref.1, bf16[2048]{0:T(1024)(128)(2,1)} %ffn_gain_ref.1, f32[16]{0:T(128)} %bias_ref.1, s32[6,16]{1,0:T(8,128)} %bitcast.10, ...), custom_call_target="tpu_custom_call" | custom-call | tf_op jit(solution)/shard_map/pallas_call | solution.py:577
  56.1 0.6 %shard_map.202 = (bf16[16,2048]{1,0:T(8,128)(2,1)}, bf16[16,64]{1,0:T(8,128)(2,1)}, bf16[16,64]{1,0:T(8,128)(2,1)}, f32[16,16]{1,0:T(8,128)}) custom-call(bf16[16,2048]{1,0:T(8,128)(2,1)S(1)} %get-tuple-element.12.refs_0_, bf16[16,64]{1,0:T(8,128)(2,1)S(1)} %get-tuple-element.13.refs_1_, bf16[16,64]{1,0:T(8,128)(2,1)S(1)} %get-tuple-element.14.refs_2_, ...), custom_call_target="tpu_custom_call" | custom-call | tf_op jit(solution)/shard_map/pallas_call | solution.py:654

commit v5 on v4

--- a/solution.py
+++ b/solution.py
@@ -21,12 +21,12 @@
 
 
 def layer_kernel(
-    len_ref,
-    attn_gain_ref,
-    ffn_gain_ref,
-    bias_ref,
-    ids_ref,
-    scores_ref,
+    len_hbm,
+    attn_gain_hbm,
+    ffn_gain_hbm,
+    bias_hbm,
+    ids_hbm,
+    scores_hbm,
     hid_hbm,
     wq_hbm,
     wk_hbm,
@@ -43,6 +43,12 @@
     key_out,
     value_out,
     logsum_out,
+    len_ref,
+    attn_gain_ref,
+    ffn_gain_ref,
+    bias_ref,
+    ids_ref,
+    scores_ref,
     hid_ref,
     wq,
     wkvf,
@@ -56,6 +62,8 @@
     gate_col,
     own_col,
     new_val,
+    scores,
+    past_weight,
     att_rows,
     att_flat,
     att_ref,
@@ -71,6 +79,7 @@
     rounded,
     mown,
     rall,
+    all_squares,
     ss,
     ssall,
     disp,
@@ -157,6 +166,17 @@
 
     get_hid = pltpu.make_async_copy(hid_hbm, hid_ref, a_sem.at[0])
     get_hid.start()
+    small = (
+        (attn_gain_hbm, attn_gain_ref),
+        (ids_hbm, ids_ref),
+        (scores_hbm, scores_ref),
+        (ffn_gain_hbm, ffn_gain_ref),
+        (bias_hbm, bias_ref),
+        (len_hbm, len_ref),
+    )
+    get_facts = [pltpu.make_async_copy(a, b, a_sem.at[21 + n]) for n, (a, b) in enumerate(small)]
+    for copy in get_facts:
+        copy.start()
     get_q = []
     for i in range(4):
         rows = pl.ds(i * 512, 512)
@@ -195,14 +215,8 @@
         )
     pl.semaphore_signal(barrier, inc=1, device_id={"tp": o}, device_id_type=MESH)
 
-    info_ref[...] = jnp.zeros((8, 128), jnp.float32)
-    info_ref[0:TOP_K, 0:ROWS] = ids_ref[...].astype(jnp.float32)
-    shares = scores_ref[...] / jnp.sum(scores_ref[...], axis=0, keepdims=True)
-    info_ref[0:TOP_K, ROWS : 2 * ROWS] = shares
-    infoall[z] = info_ref[...]
+    get_facts[0].wait()
     gains[0] = attn_gain_ref[...].astype(jnp.float32).reshape(16, 128)
-    gains[1] = ffn_gain_ref[...].astype(jnp.float32).reshape(16, 128)
-
     get_hid.wait()
     total_sq = jnp.zeros((ROWS, 128), jnp.float32)
     for i in range(16):
@@ -260,6 +274,16 @@
         over_z(lambda d, zz: send_hid(d, zz).start())
         for load in loads:
             load.start()
+
+    greet()
+    for copy in get_facts[1:]:
+        copy.wait()
+    info_ref[...] = jnp.zeros((8, 128), jnp.float32)
+    info_ref[0:TOP_K, 0:ROWS] = ids_ref[...].astype(jnp.float32)
+    shares = scores_ref[...] / jnp.sum(scores_ref[...], axis=0, keepdims=True)
+    info_ref[0:TOP_K, ROWS : 2 * ROWS] = shares
+    infoall[z] = info_ref[...]
+    gains[1] = ffn_gain_ref[...].astype(jnp.float32).reshape(16, 128)
 
     for copy in get_small:
         copy.wait()
@@ -298,53 +322,59 @@
         rows = pl.ds(piece * 8, 8)
         return z_copy(piece, att_ref.at[rows], aall.at[(d % 2) * 4 + pair, rows], zz)
 
-    for s in range(ROWS):
-        if s == 4:
-            greet()
-        if s % 4 == 0:
-            for copy in get_cache[s // 4]:
+    for piece in range(2):
+        for group in get_cache[2 * piece : 2 * piece + 2]:
+            for copy in group:
                 copy.wait()
-        rows = slice(s * 16, (s + 1) * 16)
-        q_s = heads_q[rows, :]
-        scores = jnp.dot(q_s, keys[s], preferred_element_type=jnp.float32) * score_scale
-        length = len_ref[s]
-        sums = logsum[s]
-        last = jnp.sum(jnp.where(position == length - 1, sums, 0.0), axis=-1, keepdims=True)
-        forget = jnp.sum(
-            jnp.where(diagonal, jnp.broadcast_to(gate_col[s : s + 1, :], (16, 16)), 0.0), axis=-1, keepdims=True
-        )
-        new_sum = last + forget
-        logsum_out[s : s + 1, :] = jnp.sum(
-            jnp.where(diagonal, jnp.broadcast_to(new_sum, (16, 16)), 0.0), axis=0, keepdims=True
-        )
-        scores = jnp.where(position < length, scores + new_sum - sums, -jnp.inf)
-        own_score = (
-            jnp.sum(q_s.astype(jnp.float32) * own_col[s : s + 1, :], axis=-1, keepdims=True) * score_scale
-        )
-        top = jnp.maximum(jnp.max(scores, axis=-1, keepdims=True), own_score)
-        past = jnp.exp(scores - top)
-        own_exp = jnp.exp(own_score - top)
-        share = 1.0 / (jnp.sum(past, axis=-1, keepdims=True) + own_exp)
-        past_weight = (past * share).astype(jnp.bfloat16)
-        own_weight = (own_exp * share).astype(jnp.bfloat16).astype(jnp.float32)
-        attended = lax.dot_general(
-            past_weight, values[s], (((1,), (1,)), ((), ())), preferred_element_type=jnp.float32
-        )
-        att_rows[rows, :] = (attended + own_weight * new_val[s : s + 1, :]).astype(jnp.bfloat16)
-        if s % 8 == 7:
-            piece = s // 8
-            wide = lax.dot_general(
-                att_rows[piece * 128 : (piece + 1) * 128, :],
-                fold,
-                (((1,), (1,)), ((), ())),
-                preferred_element_type=jnp.float32,
-            )
-            for i in range(8):
-                att_flat[i : i + 1, :] = jnp.sum(
-                    jnp.where(own_lanes, wide[i * 16 : (i + 1) * 16, :], 0.0), axis=0, keepdims=True
-                )
-            att_ref[piece * 8 : (piece + 1) * 8, :] = att_flat[...].astype(jnp.bfloat16)
-            over_z(lambda d, zz, piece=piece: send_att(piece, d, zz).start())
+        tops, own_scores, own_weights = [], [], []
+        for i in range(8):
+            s = piece * 8 + i
+            q_s = heads_q[s * 16 : (s + 1) * 16, :]
+            raw = jnp.dot(q_s, keys[s], preferred_element_type=jnp.float32) * score_scale
+            length = len_ref[s]
+            sums = logsum[s]
+            last = jnp.sum(jnp.where(position == length - 1, sums, 0.0), axis=-1, keepdims=True)
+            forget = jnp.sum(
+                jnp.where(diagonal, jnp.broadcast_to(gate_col[s : s + 1, :], (16, 16)), 0.0),
+                axis=-1,
+                keepdims=True,
+            )
+            new_sum = last + forget
+            logsum_out[s : s + 1, :] = jnp.sum(
+                jnp.where(diagonal, jnp.broadcast_to(new_sum, (16, 16)), 0.0), axis=0, keepdims=True
+            )
+            masked = jnp.where(position < length, raw + new_sum - sums, -jnp.inf)
+            own_score = (
+                jnp.sum(q_s.astype(jnp.float32) * own_col[s : s + 1, :], axis=-1, keepdims=True) * score_scale
+            )
+            scores[i] = masked
+            own_scores.append(own_score)
+            tops.append(jnp.maximum(jnp.max(masked, axis=-1, keepdims=True), own_score))
+        for i in range(8):
+            past = jnp.exp(scores[i] - tops[i])
+            own_exp = jnp.exp(own_scores[i] - tops[i])
+            share = 1.0 / (jnp.sum(past, axis=-1, keepdims=True) + own_exp)
+            past_weight[i] = (past * share).astype(jnp.bfloat16)
+            own_weights.append((own_exp * share).astype(jnp.bfloat16).astype(jnp.float32))
+        for i in range(8):
+            s = piece * 8 + i
+            attended = lax.dot_general(
+                past_weight[i], values[s], (((1,), (1,)), ((), ())), preferred_element_type=jnp.float32
+            )
+            attended = attended + own_weights[i] * new_val[s : s + 1, :]
+            att_rows[s * 16 : (s + 1) * 16, :] = attended.astype(jnp.bfloat16)
+        wide = lax.dot_general(
+            att_rows[piece * 128 : (piece + 1) * 128, :],
+            fold,
+            (((1,), (1,)), ((), ())),
+            preferred_element_type=jnp.float32,
+        )
+        for i in range(8):
+            att_flat[i : i + 1, :] = jnp.sum(
+                jnp.where(own_lanes, wide[i * 16 : (i + 1) * 16, :], 0.0), axis=0, keepdims=True
+            )
+        att_ref[piece * 8 : (piece + 1) * 8, :] = att_flat[...].astype(jnp.bfloat16)
+        over_z(lambda d, zz, piece=piece: send_att(piece, d, zz).start())
     over_z(lambda d, zz: send_info(d, zz).start())
     aall[pair] = att_ref[...]
     wholes = ((gate_v, gate_p), (up_v, up_p), (down_v, down_p))
@@ -357,54 +387,61 @@
     get_wo.wait()
     with jax.named_scope("b_w"):
         p_wait(0, wall.at[pl.ds(0, 15)])
-    with jax.named_scope("c_att"):
-        for piece in range(2):
+    def send_rounded(j, piece, d, zz):
+        return z_copy(4 + 6 * piece + j, rounded.at[t, piece, (d + j) % 2], rall.at[j, z, piece], zz)
+
+    def send_mixed(d, zz):
+        return z_copy(6, mixed.at[t, (d % 2) * 4 + zz // 2], mown.at[z], zz)
+
+    def send_ss(d, zz):
+        return z_copy(8, ss.at[d % 2], ssall.at[z], zz)
+
+    gives = [t_copy(8 * piece, part.at[piece], part_in.at[piece]) for piece in range(2)]
+    for piece in range(2):
+        eight = slice(piece * 8, (piece + 1) * 8)
+        with jax.named_scope(f"c_att#p={piece}"):
             z_wait(piece, aall.at[pl.ds(0, 7), pl.ds(piece * 8, 8)])
-
-    att = aall[...].reshape(NZ * ROWS, HALF)
-    for h in range(2):
-        weights = wall[h * 8 : (h + 1) * 8].reshape(128, HALF)
-        part[h] = lax.dot_general(att, weights, (((1,), (1,)), ((), ())), preferred_element_type=jnp.float32)
-    give = t_copy(0, part, part_in)
-    give.start()
+        att = aall[:, eight, :].reshape(64, HALF)
+        for h in range(2):
+            weights = wall[h * 8 : (h + 1) * 8].reshape(128, HALF)
+            part[piece, h] = lax.dot_general(
+                att, weights, (((1,), (1,)), ((), ())), preferred_element_type=jnp.float32
+            )
+        gives[piece].start()
     with jax.named_scope("e_hid"):
         z_wait(2, hcol.at[pl.ds(0, 7)])
-    with jax.named_scope("e_give"):
-        give.wait_recv()
-    squares = jnp.zeros((NZ * ROWS, 128), jnp.float32)
-    for h in range(2):
-        mixed_now = (part[h] + part_in[h]).astype(jnp.bfloat16)
-        hid_now = hcol[:, :, h * 128 : (h + 1) * 128].reshape(NZ * ROWS, 128).astype(jnp.float32)
-        residual = hid_now + mixed_now.astype(jnp.float32)
-        squares = squares + residual * residual
-        mixed[h] = mixed_now.reshape(8, ROWS, 128)
-        rounded[h] = residual.astype(jnp.bfloat16).reshape(2, 4, ROWS, 128)
-
-    def send_rounded(j, d, zz):
-        return z_copy(4 + j, rounded.at[t, (d + j) % 2], rall.at[j, z], zz)
-
-    def send_mixed(d, zz):
-        return z_copy(6, mixed.at[t, (d % 2) * 4 + zz // 2], mown.at[z], zz)
-
-    def send_ss(d, zz):
-        return z_copy(8, ss.at[d % 2], ssall.at[z], zz)
-
-    over_z(lambda d, zz: send_rounded(0, d, zz).start())
-    sums = lax.dot_general(
-        jnp.ones((8, 128), jnp.float32),
-        squares,
-        (((1,), (1,)), ((), ())),
-        precision=lax.Precision.HIGHEST,
-        preferred_element_type=jnp.float32,
-    )
-    ss[0] = sums
-    ss[1] = pltpu.roll(sums, 64, 1)
-    over_z(lambda d, zz: send_ss(d, zz).start())
-    over_z(lambda d, zz: send_rounded(1, d, zz).start())
+    for piece in range(2):
+        eight = slice(piece * 8, (piece + 1) * 8)
+        with jax.named_scope(f"e_give#p={piece}"):
+            gives[piece].wait_recv()
+        squares = jnp.zeros((64, 128), jnp.float32)
+        for h in range(2):
+            mixed_now = (part[piece, h] + part_in[piece, h]).astype(jnp.bfloat16)
+            hid_now = hcol[:, eight, h * 128 : (h + 1) * 128].reshape(64, 128).astype(jnp.float32)
+            residual = hid_now + mixed_now.astype(jnp.float32)
+            squares = squares + residual * residual
+            mixed[h, :, eight, :] = mixed_now.reshape(8, 8, 128)
+            rounded[h, piece] = residual.astype(jnp.bfloat16).reshape(2, 4, 8, 128)
+        for j in range(2):
+            all_squares[j, piece] = squares[j * 32 : (j + 1) * 32]
+        over_z(lambda d, zz, piece=piece: send_rounded(0, piece, d, zz).start())
+        if piece == 1:
+            sums = lax.dot_general(
+                jnp.ones((8, 128), jnp.float32),
+                all_squares[...].reshape(128, 128),
+                (((1,), (1,)), ((), ())),
+                precision=lax.Precision.HIGHEST,
+                preferred_element_type=jnp.float32,
+            )
+            ss[0] = sums
+            ss[1] = pltpu.roll(sums, 64, 1)
+            over_z(lambda d, zz: send_ss(d, zz).start())
+        over_z(lambda d, zz, piece=piece: send_rounded(1, piece, d, zz).start())
     over_z(lambda d, zz: send_mixed(d, zz).start())
     ssall[z] = ss[0]
     for j in range(2):
-        rall[j, z] = rounded[t, j]
+        for piece in range(2):
+            rall[j, z, piece] = rounded[t, piece, j]
     mown[z] = mixed[t, pair]
 
     with jax.named_scope("d_info"):
@@ -414,10 +451,14 @@
     weights_of = jnp.zeros((8, 128), jnp.float32)
     for zz in range(NZ):
         tile = infoall[zz]
-        place = (lax.rem(z + zz, 2) * 4 + zz // 2) * ROWS
-        routes = routes + pltpu.roll(jnp.where(lane < ROWS, tile, 0.0), place, 1)
-        tile = jnp.where((lane >= ROWS) & (lane < 2 * ROWS), tile, 0.0)
-        weights_of = weights_of + pltpu.roll(tile, lax.rem(place + 128 - ROWS, 128), 1)
+        place = lax.rem(z + zz, 2) * 64 + (zz // 2) * 8
+        for piece in range(2):
+            low = piece * 8
+            one = jnp.where((lane >= low) & (lane < low + 8), tile, 0.0)
+            routes = routes + pltpu.roll(one, lax.rem(place + 32 * piece + 128 - low, 128), 1)
+            low = ROWS + piece * 8
+            one = jnp.where((lane >= low) & (lane < low + 8), tile, 0.0)
+            weights_of = weights_of + pltpu.roll(one, lax.rem(place + 32 * piece + 128 - low, 128), 1)
     row = lax.broadcasted_iota(jnp.int32, (256, 128), 0)
     token = lax.broadcasted_iota(jnp.int32, (256, 128), 1)
     expert = (lax.rem(row, 128) // 8 + z * PLANE).astype(jnp.float32)
@@ -429,10 +470,13 @@
         scale = scale + jnp.where(hit, weights_of[j : j + 1, :], 0.0)
     first = lax.broadcasted_iota(jnp.int32, (128, 128), 0)
     second = lax.broadcasted_iota(jnp.int32, (128, 128), 1)
-    ahead = jnp.where((first // ROWS == second // ROWS) & (first < second), 1.0, 0.0).astype(jnp.bfloat16)
+    same = (first // 64 == second // 64) & (lax.rem(first, 32) // 8 == lax.rem(second, 32) // 8)
+    place_first = lax.rem(first, 64) // 32 * 8 + lax.rem(first, 8)
+    place_second = lax.rem(second, 64) // 32 * 8 + lax.rem(second, 8)
+    ahead = jnp.where(same & (place_first < place_second), 1.0, 0.0).astype(jnp.bfloat16)
     rank = jnp.dot(named.astype(jnp.bfloat16), ahead, preferred_element_type=jnp.float32)
     slot = lax.rem(row, 2).astype(jnp.float32)
-    here = (row // 128) * 4 + lax.rem(row, 8) // 2 == token // ROWS
+    here = (row // 128 == token // 64) & (lax.rem(row, 8) // 2 == lax.rem(token, 32) // 8)
     pick = jnp.where(here & (rank == slot), named, 0.0)
     combine = jnp.transpose(pick * scale)
     picks = [pick[0:128, 0:64].astype(jnp.bfloat16), pick[128:256, 64:128].astype(jnp.bfloat16)]
@@ -449,7 +493,8 @@
         with jax.named_scope(f"g_mixed#j={j}"):
             if j == 0:
                 z_wait(8, ssall.at[pl.ds(0, 7)])
-            z_wait(4 + j, rall.at[j, pl.ds(0, 7)])
+            for piece in range(2):
+                z_wait(4 + 6 * piece + j, rall.at[j, pl.ds(0, 7), piece])
         if j == 0:
             inverse = lax.rsqrt(jnp.sum(ssall[...], axis=0)[0:1, :] * (1.0 / WIDE) + epsilon)
             factor = jnp.sum(pick * inverse, axis=-1, keepdims=True)
@@ -521,7 +566,9 @@
             outs = back[j, q].reshape(128, 512)
             total = jnp.dot(combine_high[j], outs, preferred_element_type=jnp.float32)
             total = total + jnp.dot(combine_low[j], outs, preferred_element_type=jnp.float32)
-            psum[j, q] = total.astype(jnp.bfloat16).reshape(4, ROWS, 512)
+            for piece in range(2):
+                half = total[piece * 32 : (piece + 1) * 32]
+                psum[j, q, :, piece * 8 : (piece + 1) * 8, :] = half.astype(jnp.bfloat16).reshape(4, 8, 512)
             for d in z_steps:
                 if d % 2 == j:
                     send_sum(j, q, d, lax.rem(z + d, NZ)).start()
@@ -552,12 +599,14 @@
             aall.at[pl.ds(0, 7), pl.ds(8, 8)],
             hcol.at[pl.ds(0, 7)],
             infoall.at[pl.ds(0, 7)],
-            rall.at[0, pl.ds(0, 7)],
-            rall.at[1, pl.ds(0, 7)],
+            rall.at[0, pl.ds(0, 7), 0],
+            rall.at[1, pl.ds(0, 7), 0],
             mown.at[pl.ds(0, 7)],
             tsum.at[0, pl.ds(0, 7)],
             ssall.at[pl.ds(0, 7)],
             tsum.at[1, pl.ds(0, 7)],
+            rall.at[0, pl.ds(0, 7), 1],
+            rall.at[1, pl.ds(0, 7), 1],
         )
         for phase, ref in enumerate(sent):
             z_copy(phase, ref, ref, next_z).wait_send()
@@ -565,7 +614,7 @@
         sent += [ret.at[h, q, pl.ds(0, 15)] for h in range(2) for q in range(2)]
         for phase, ref in enumerate(sent):
             p_copy(phase, ref, ref, next_p, 0, t).wait_send()
-        for give_one in [give, give_u, give_rows, give_ret(0), give_ret(1)] + swaps:
+        for give_one in [give_u, give_rows, give_ret(0), give_ret(1)] + gives + swaps:
             give_one.wait_send()
 
 
@@ -582,9 +631,15 @@
             pltpu.VMEM((ROWS, HD), bf16),
             pltpu.VMEM((ROWS, 16), f32),
         ),
-        in_specs=[pl.BlockSpec(memory_space=pltpu.SMEM)] + [vmem] * 5 + [hbm] * 12,
+        in_specs=[hbm] * 18,
         out_specs=(vmem,) * 4,
         scratch_shapes=[
+            pltpu.SMEM((ROWS,), jnp.int32),
+            pltpu.VMEM((WIDE,), bf16),
+            pltpu.VMEM((WIDE,), bf16),
+            pltpu.VMEM((16,), f32),
+            pltpu.VMEM((TOP_K, ROWS), jnp.int32),
+            pltpu.VMEM((TOP_K, ROWS), f32),
             pltpu.VMEM((ROWS, WIDE), bf16),
             pltpu.VMEM((WIDE, HALF), bf16),
             pltpu.VMEM((144, WIDE), bf16),
@@ -598,6 +653,8 @@
             pltpu.VMEM((ROWS, 16), f32),
             pltpu.VMEM((ROWS, HD), f32),
             pltpu.VMEM((ROWS, HD), f32),
+            pltpu.VMEM((8, 16, 1024), f32),
+            pltpu.VMEM((8, 16, 1024), bf16),
             pltpu.VMEM((256, HD), bf16),
             pltpu.VMEM((8, HALF), f32),
             pltpu.VMEM((ROWS, HALF), bf16),
@@ -607,12 +664,13 @@
             pltpu.VMEM((PLANE, ROWS, HALF), bf16),
             pltpu.VMEM((8, ROWS, HALF), bf16),
             pltpu.VMEM((8, ROWS, 256), bf16),
-            pltpu.VMEM((2, NZ * ROWS, 128), f32),
-            pltpu.VMEM((2, NZ * ROWS, 128), f32),
+            pltpu.VMEM((2, 2, 64, 128), f32),
+            pltpu.VMEM((2, 2, 64, 128), f32),
             pltpu.VMEM((2, 8, ROWS, 128), bf16),
-            pltpu.VMEM((2, 2, 4, ROWS, 128), bf16),
+            pltpu.VMEM((2, 2, 2, 4, 8, 128), bf16),
             pltpu.VMEM((NZ, ROWS, 128), bf16),
-            pltpu.VMEM((2, NZ, 4, ROWS, 128), bf16),
+            pltpu.VMEM((2, NZ, 2, 4, 8, 128), bf16),
+            pltpu.VMEM((2, 2, 32, 128), f32),
             pltpu.VMEM((2, 8, 128), f32),
             pltpu.VMEM((NZ, 8, 128), f32),
             pltpu.VMEM((2, PLANE, 8, HALF), bf16),
@@ -629,14 +687,14 @@
             pltpu.VMEM((2, NZ, ROWS, 512), bf16),
             pltpu.VMEM((ROWS, HALF), bf16),
             pltpu.VMEM((ROWS, HALF), bf16),
-            dma((10,)),
-            dma((10,)),
+            dma((12,)),
+            dma((12,)),
             dma((7,)),
             dma((7,)),
-            dma((8,)),
-            dma((8,)),
+            dma((9,)),
+            dma((9,)),
             dma((3,)),
-            dma((21,)),
+            dma((27,)),
         ],
         compiler_params=pltpu.CompilerParams(
             collective_id=0, has_side_effects=True, vmem_limit_bytes=56 * 1024 * 1024

time: 56.9 us -> 56.2 us (0.988)
  Pallas kernels: 56.1 us -> 55.5 us
    pallas_call x1, Pallas kernels: 55.5 us -> 54.8 us  [layer(): pl.pallas_call(layer_kernel, out_shape=(pltpu.VMEM((ROWS, WIDE), bf16), p...]
where the time goes in v5:
time: 56.2 us; the launch traced here: 56.1 us
  Pallas kernels  55.5 us (99%)
  between operations  0.65 us (1%)
    pallas_call x1, Pallas kernels, layer(): pl.pallas_call(layer_kernel, out_shape=(pltpu.VMEM((ROWS, WIDE), bf16), p...  54.8 us

profile of v5, /device:TPU:1, one launch (start us, length us, event | category | flops | bytes accessed | tf_op | source)
XLA Modules:
  0.0 56.1 jit_solution(4442218884174491267)
XLA Ops:
  0.6 54.8 %shard_map.201 = (bf16[16,2048]{1,0:T(8,128)(2,1)S(1)}, bf16[16,64]{1,0:T(8,128)(2,1)S(1)}, bf16[16,64]{1,0:T(8,128)(2,1)S(1)}, f32[16,16]{1,0:T(8,128)S(1)}) custom-call(s32[16]{0:T(128)} %len_hbm.1, bf16[2048]{0:T(1024)(128)(2,1)} %attn_gain_hbm.1, bf16[2048]{0:T(1024)(128)(2,1)} %ffn_gain_hbm.1, f32[16]{0:T(128)} %bias_hbm.1, s32[6,16]{1,0:T(8,128)} %bitcast.10, ...), custom_call_target="tpu_custom_call" | custom-call | tf_op jit(solution)/shard_map/pallas_call | solution.py:626
  55.5 0.6 %shard_map.202 = (bf16[16,2048]{1,0:T(8,128)(2,1)}, bf16[16,64]{1,0:T(8,128)(2,1)}, bf16[16,64]{1,0:T(8,128)(2,1)}, f32[16,16]{1,0:T(8,128)}) custom-call(bf16[16,2048]{1,0:T(8,128)(2,1)S(1)} %get-tuple-element.12.refs_0_, bf16[16,64]{1,0:T(8,128)(2,1)S(1)} %get-tuple-element.13.refs_1_, bf16[16,64]{1,0:T(8,128)(2,1)S(1)} %get-tuple-element.14.refs_2_, ...), custom_call_target="tpu_custom_call" | custom-call | tf_op jit(solution)/shard_map/pallas_call | solution.py:712

commit v6 on v5

--- a/solution.py
+++ b/solution.py
@@ -559,8 +559,8 @@
 
     for q in range(2):
         give_ret(q).wait_recv()
-    for j in range(2):
-        for q in range(2):
+    for q in range(2):
+        for j in range(2):
             with jax.named_scope(f"m_ret#j={j}#q={q}"):
                 p_wait(3 + j * 2 + q, back.at[j, q, pl.ds(0, 15)])
             outs = back[j, q].reshape(128, 512)

time: 56.2 us -> 54.3 us (0.966)
  Pallas kernels: 55.5 us -> 53.6 us
    pallas_call x1, Pallas kernels: 54.8 us -> 52.9 us  [layer(): pl.pallas_call(layer_kernel, out_shape=(pltpu.VMEM((ROWS, WIDE), bf16), p...]
where the time goes in v6:
time: 54.3 us; the launch traced here: 54.2 us
  Pallas kernels  53.6 us (99%)
  between operations  0.65 us (1%)
    pallas_call x1, Pallas kernels, layer(): pl.pallas_call(layer_kernel, out_shape=(pltpu.VMEM((ROWS, WIDE), bf16), p...  52.9 us

profile of v6, /device:TPU:1, one launch (start us, length us, event | category | flops | bytes accessed | tf_op | source)
XLA Modules:
  0.0 54.2 jit_solution(13066523528625144312)
XLA Ops:
  0.6 52.9 %shard_map.201 = (bf16[16,2048]{1,0:T(8,128)(2,1)S(1)}, bf16[16,64]{1,0:T(8,128)(2,1)S(1)}, bf16[16,64]{1,0:T(8,128)(2,1)S(1)}, f32[16,16]{1,0:T(8,128)S(1)}) custom-call(s32[16]{0:T(128)} %len_hbm.1, bf16[2048]{0:T(1024)(128)(2,1)} %attn_gain_hbm.1, bf16[2048]{0:T(1024)(128)(2,1)} %ffn_gain_hbm.1, f32[16]{0:T(128)} %bias_hbm.1, s32[6,16]{1,0:T(8,128)} %bitcast.10, ...), custom_call_target="tpu_custom_call" | custom-call | tf_op jit(solution)/shard_map/pallas_call | solution.py:626
  53.6 0.6 %shard_map.202 = (bf16[16,2048]{1,0:T(8,128)(2,1)}, bf16[16,64]{1,0:T(8,128)(2,1)}, bf16[16,64]{1,0:T(8,128)(2,1)}, f32[16,16]{1,0:T(8,128)}) custom-call(bf16[16,2048]{1,0:T(8,128)(2,1)S(1)} %get-tuple-element.12.refs_0_, bf16[16,64]{1,0:T(8,128)(2,1)S(1)} %get-tuple-element.13.refs_1_, bf16[16,64]{1,0:T(8,128)(2,1)S(1)} %get-tuple-element.14.refs_2_, ...), custom_call_target="tpu_custom_call" | custom-call | tf_op jit(solution)/shard_map/pallas_call | solution.py:712
